TPU v7x, 512 devices: a whole 4x4x16 slice. The times are simulated.
512 devices in a mesh: fs: 128 (over z, x, core), tp: 4 (over y).
Axes of the slice: x: 4, y: 4, z: 16, core: 2. Of those that a mesh axis runs over, the one named last changes fastest.
Arguments:
- q_latent: bfloat16 [98304, 512], P('fs'), may hold values from -24 to 24
- q_grad: bfloat16 [98304, 3072], P('fs', 'tp'), may hold values from -6 to 6
- uq_master: float32 [512, 3072], P('fs', 'tp'), may hold values from -6 to 6
- uq_basis: bfloat16 [512, 256], P('fs'), may hold values from -4 to 4
- uq_first: float32 [256, 3072], P('fs', 'tp'), may hold values from -3 to 3
- uq_second: float32 [256, 3072], P('fs', 'tp'), may hold values from 0.1 to 1
- kv_latent: bfloat16 [98304, 512], P('fs'), may hold values from -24 to 24
- k_grad: bfloat16 [98304, 2048], P('fs', 'tp'), may hold values from -6 to 6
- uk_master: float32 [512, 2048], P('fs', 'tp'), may hold values from -6 to 6
- uk_basis: bfloat16 [512, 256], P('fs'), may hold values from -4 to 4
- uk_first: float32 [256, 2048], P('fs', 'tp'), may hold values from -3 to 3
- uk_second: float32 [256, 2048], P('fs', 'tp'), may hold values from 0.1 to 1
Outputs:
- uq_first_new: float32 [256, 3072], P('fs', 'tp')
- uq_second_new: float32 [256, 3072], P('fs', 'tp')
- uq_step: float32 [512, 3072], P('fs', 'tp')
- uq_copy: bfloat16 [512, 3072], P(None, 'tp')
- uk_first_new: float32 [256, 2048], P('fs', 'tp')
- uk_second_new: float32 [256, 2048], P('fs', 'tp')
- uk_step: float32 [512, 2048], P('fs', 'tp')
- uk_copy: bfloat16 [512, 2048], P(None, 'tp')
All inputs are finite; a program needn't handle non-finite values.
Results may differ from a plain program's by a relative error of at most 0.0071.
Values may be sent and summed in bfloat16 or wider, within the bound.
A program may use at most 64 MiB of HBM per device.

v0:
```python
import jax
import jax.numpy as jnp
from jax import lax
from jax.sharding import Mesh
from jax.sharding import PartitionSpec as P

FS = ("fs_0", "fs_1", "fs_2")


first_decay = 0.8
second_decay = 0.9
step_size = 0.5
mean_guard = 1e-06
root_guard = 1e-08


def from_everyone(x, axis):
    copies = jnp.broadcast_to(x, (lax.axis_size(axis), *x.shape))
    return lax.all_to_all(copies, axis, split_axis=0, concat_axis=0, tiled=True)


def laid_out(blocks, dim):
    shape = list(blocks.shape[1:])
    shape[dim] *= blocks.shape[0]
    return jnp.moveaxis(blocks, 0, dim).reshape(shape)


def whole_of(x, axes, dim):
    far, near = axes
    blocks = from_everyone(from_everyone(x, far), near)
    return laid_out(blocks.swapaxes(0, 1).reshape(-1, *x.shape), dim)


def in_one_piece(arrays, axis, dim, along):
    widths = [a.shape[along] for a in arrays]
    both = jnp.concatenate(arrays, axis=along)
    filled = whole_of(both, axis, dim)
    return tuple(jnp.split(filled, [sum(widths[:k]) for k in range(1, len(widths))], axis=along))


def split_up(x, dim, devices):
    shape = x.shape
    blocks = x.reshape(*shape[:dim], devices, shape[dim] // devices, *shape[dim + 1 :])
    return jnp.moveaxis(blocks, dim, 0)


def sum_at_owner(x, axis, dim):
    blocks = split_up(x, dim, lax.axis_size(axis))
    arrived = lax.all_to_all(blocks, axis, split_axis=0, concat_axis=0, tiled=True)
    return arrived.astype(jnp.float32).sum(axis=0)


def sum_in_two_steps(x, axes, dim):
    far, near = axes
    own = sum_at_owner(split_up(x, dim, lax.axis_size(far)), near, dim + 1)
    return jnp.sum(
        lax.all_to_all(own.astype(jnp.bfloat16), far, 0, 0, tiled=True).astype(jnp.float32), axis=0
    )


def over_copies(x, axis):
    return from_everyone(x, axis).sum(axis=0)


def one_axis_at_a_time(x, axes):
    far, near = axes
    nearer = over_copies(x, near)
    return over_copies(nearer, far)


def across_tokens(left, right):
    return lax.dot_general(
        left, right, (((0,), (0,)), ((), ())), preferred_element_type=jnp.float32
    )


def across_latent(left, right):
    return lax.dot_general(
        left,
        right,
        (((0,), (0,)), ((), ())),
        precision=lax.Precision.HIGHEST,
        preferred_element_type=jnp.float32,
    )


def moment_update(scaled, first_old, second_old):
    first_new = first_decay * first_old + (1.0 - first_decay) * scaled
    second_new = second_decay * second_old + (1.0 - second_decay) * scaled * scaled
    heading = (first_new / (jnp.sqrt(second_new) + root_guard)).astype(jnp.bfloat16)
    return (first_new, second_new, heading)


def body(
    q_latent,
    q_grad,
    uq_master,
    uq_basis,
    uq_first,
    uq_second,
    kv_latent,
    k_grad,
    uk_master,
    uk_basis,
    uk_first,
    uk_second,
):
    q_width = q_grad.shape[1]
    q_whole, k_whole = in_one_piece((uq_basis, uk_basis), (("fs_0", "fs_1"), "fs_2"), 0, 1)
    q_factor = q_whole.astype(jnp.float32)
    k_factor = k_whole.astype(jnp.float32)
    q_partial = across_tokens(q_latent, q_grad)
    k_partial = across_tokens(kv_latent, k_grad)
    projected = sum_in_two_steps(
        jnp.concatenate(
            [across_latent(q_factor, q_partial), across_latent(k_factor, k_partial)], axis=1
        ).astype(jnp.bfloat16),
        (("fs_0", "fs_1"), "fs_2"),
        0,
    )
    squares_sum = one_axis_at_a_time(
        jnp.sum(projected * projected), (("fs_0", "fs_1"), ("fs_2", "tp"))
    )
    entry_count = projected.shape[0] * projected.shape[1] * lax.axis_size(FS) * lax.axis_size("tp")
    root_mean = jnp.sqrt(squares_sum / entry_count + mean_guard)
    scaled = projected / root_mean
    uq_first_new, uq_second_new, q_heading = moment_update(scaled[:, :q_width], uq_first, uq_second)
    uk_first_new, uk_second_new, k_heading = moment_update(scaled[:, q_width:], uk_first, uk_second)
    q_dir, k_dir = in_one_piece((q_heading, k_heading), (("fs_0", "fs_1"), "fs_2"), 0, 1)
    uq_step = jnp.dot(uq_basis, q_dir, preferred_element_type=jnp.float32)
    uk_step = jnp.dot(uk_basis, k_dir, preferred_element_type=jnp.float32)
    q_fresh = (uq_master - step_size * uq_step).astype(jnp.bfloat16)
    k_fresh = (uk_master - step_size * uk_step).astype(jnp.bfloat16)
    uq_copy, uk_copy = in_one_piece((q_fresh, k_fresh), (("fs_0", "fs_1"), "fs_2"), 0, 1)
    return (
        uq_first_new,
        uq_second_new,
        uq_step,
        uq_copy,
        uk_first_new,
        uk_second_new,
        uk_step,
        uk_copy,
    )


def solution(mesh):
    finer = Mesh(mesh.devices.reshape(16, 4, 2, mesh.shape["tp"]), ("fs_0", "fs_1", "fs_2", "tp"))
    in_specs = (
        P(FS, None),
        P(FS, "tp"),
        P(FS, "tp"),
        P(FS, None),
        P(FS, "tp"),
        P(FS, "tp"),
        P(FS, None),
        P(FS, "tp"),
        P(FS, "tp"),
        P(FS, None),
        P(FS, "tp"),
        P(FS, "tp"),
    )
    out_specs = (
        P(FS, "tp"),
        P(FS, "tp"),
        P(FS, "tp"),
        P(None, "tp"),
        P(FS, "tp"),
        P(FS, "tp"),
        P(FS, "tp"),
        P(None, "tp"),
    )
    return jax.shard_map(body, mesh=finer, in_specs=in_specs, out_specs=out_specs, check_vma=False)
```

profile of v0, /device:TPU:1, one launch (start us, length us, event | category | flops | bytes accessed | tf_op | source)
XLA Modules:
  0.0 212.7 jit_solution(278243348184979062)
XLA Ops:
  0.6 0.8 pad_maximum_fusion.3
  1.4 0.8 broadcast_in_dim.24
  2.2 19.1 %all-to-all-start = ((bf16[64,4,512]{2,1,0:T(4,128)(2,1)}), bf16[64,4,512]{2,1,0:T(4,128)(2,1)S(1)}, u32[]{:S(2)}, u32[]{:S(2)}) async-start(bf16[64,4,512]{2,1,0:T(4,128)(2,1)} %broadcast_in_dim.24), calls=%async_computation | async-start | bytes 524288 | tf_op jit(solution)/shard_map/all_to_all | solution.py:19
  21.3 2.0 fusion.11
  23.4 2.0 fusion.10
  25.4 15.4 %all-to-all-done = bf16[64,4,512]{2,1,0:T(4,128)(2,1)S(1)} async-done(((bf16[64,4,512]{2,1,0:T(4,128)(2,1)}), bf16[64,4,512]{2,1,0:T(4,128)(2,1)S(1)}, u32[]{:S(2)}, u32[]{:S(2)}) %all-to-all-start) | async-done | bytes 262176 | tf_op jit(solution)/shard_map/all_to_all | solution.py:19
  40.9 7.7 %all_to_all.52 = bf16[2,64,4,512]{3,2,1,0:T(4,128)(2,1)S(1)} all-to-all(bf16[2,64,4,512]{3,2,1,0:T(4,128)(2,1)S(1)} %broadcast_in_dim.25), channel_id=1, replica_groups=mesh['fs_0'=16,'fs_1'=4,'fs_2'=2,'tp'=4] {'fs_2'}, dimensions={0} | all-to-all | bytes 1048576 | tf_op jit(solution)/shard_map/all_to_all | solution.py:19
  49.0 2.3 %convolution_convert_fusion = bf16[256,768]{1,0:T(8,128)(2,1)S(1)} fusion(f32[512,768]{1,0:T(8,128)} %fusion.10, bf16[512,512]{1,0:T(8,128)(2,1)S(1)} %reshape_reshape.10), kind=kOutput, calls=%fused_computation | convolution fusion | flops 1208156160 | bytes 2228224 | tf_op jit(solution)/shard_map/dot_general | solution.py:78
  51.5 0.7 convolution_convert_fusion.1
  52.3 0.6 copy_bitcast_fusion
  52.8 4.3 %all_to_all.53 = bf16[2,64,2,1280]{3,2,1,0:T(2,128)(2,1)S(1)} all-to-all(bf16[2,64,2,1280]{3,2,1,0:T(2,128)(2,1)S(1)} %copy_bitcast_fusion), channel_id=1, replica_groups=mesh['fs_0'=16,'fs_1'=4,'fs_2'=2,'tp'=4] {'fs_2'}, dimensions={0} | all-to-all | bytes 1310720 | tf_op jit(solution)/shard_map/all_to_all | solution.py:49
  57.1 1.4 reduce_sum.48
  58.5 27.2 %all_to_all.54 = bf16[64,2,1280]{2,1,0:T(2,128)(2,1)S(1)} all-to-all(bf16[64,2,1280]{2,1,0:T(2,128)(2,1)S(1)} %reduce_sum.48), channel_id=1, replica_groups=mesh['fs_0'=16,'fs_1'=4,'fs_2'=2,'tp'=4] {'fs_0','fs_1'}, dimensions={0} | all-to-all | bytes 655360 | tf_op jit(solution)/shard_map/all_to_all | solution.py:57
  85.8 0.6 multiply_reduce_fusion
  86.4 0.6 broadcast_in_dim.26
  87.0 12.1 %all_to_all.55 = f32[8,1,1]{2,1,0:T(1,128)S(1)} all-to-all(f32[8,1,1]{2,1,0:T(1,128)S(1)} %broadcast_in_dim.26), channel_id=1, replica_groups=mesh['fs_0'=16,'fs_1'=4,'fs_2'=2,'tp'=4] {'fs_2','tp'}, dimensions={0} | all-to-all | bytes 64 | tf_op jit(solution)/shard_map/all_to_all | solution.py:19
  99.1 0.6 reduce_sum.51
  99.8 0.7 broadcast_in_dim.27
  100.4 18.2 %all_to_all.56 = f32[64,1,1]{2,1,0:T(1,128)S(1)} all-to-all(f32[64,1,1]{2,1,0:T(1,128)S(1)} %broadcast_in_dim.27), channel_id=1, replica_groups=mesh['fs_0'=16,'fs_1'=4,'fs_2'=2,'tp'=4] {'fs_0','fs_1'}, dimensions={0} | all-to-all | bytes 512 | tf_op jit(solution)/shard_map/all_to_all | solution.py:19
  118.7 0.7 reduce_sum.52
  120.1 0.6 fusion.5
  120.7 0.6 fusion.7
  121.5 24.9 %all_to_all.57 = bf16[64,2,1280]{2,1,0:T(2,128)(2,1)S(1)} all-to-all(bf16[64,2,1280]{2,1,0:T(2,128)(2,1)S(1)} %broadcast_in_dim.28), channel_id=1, replica_groups=mesh['fs_0'=16,'fs_1'=4,'fs_2'=2,'tp'=4] {'fs_0','fs_1'}, dimensions={0} | all-to-all | bytes 655360 | tf_op jit(solution)/shard_map/all_to_all | solution.py:19
  146.7 9.0 %all_to_all.58 = bf16[2,64,2,1280]{3,2,1,0:T(2,128)(2,1)S(1)} all-to-all(bf16[2,64,2,1280]{3,2,1,0:T(2,128)(2,1)S(1)} %broadcast_in_dim.29), channel_id=1, replica_groups=mesh['fs_0'=16,'fs_1'=4,'fs_2'=2,'tp'=4] {'fs_2'}, dimensions={0} | all-to-all | bytes 1310720 | tf_op jit(solution)/shard_map/all_to_all | solution.py:19
  156.5 0.8 subtract_convert_fusion
  157.2 0.7 subtract_convert_fusion.1
  158.2 40.5 %all_to_all.59 = bf16[64,4,1280]{2,1,0:T(4,128)(2,1)S(1)} all-to-all(bf16[64,4,1280]{2,1,0:T(4,128)(2,1)S(1)} %broadcast_in_dim.30), channel_id=1, replica_groups=mesh['fs_0'=16,'fs_1'=4,'fs_2'=2,'tp'=4] {'fs_0','fs_1'}, dimensions={0} | all-to-all | bytes 1310720 | tf_op jit(solution)/shard_map/all_to_all | solution.py:19
  199.1 7.8 %all_to_all.60 = bf16[2,64,4,1280]{3,2,1,0:T(4,128)(2,1)S(1)} all-to-all(bf16[2,64,4,1280]{3,2,1,0:T(4,128)(2,1)S(1)} %broadcast_in_dim.31), channel_id=1, replica_groups=mesh['fs_0'=16,'fs_1'=4,'fs_2'=2,'tp'=4] {'fs_2'}, dimensions={0} | all-to-all | bytes 2621440 | tf_op jit(solution)/shard_map/all_to_all | solution.py:19
  206.9 1.5 copy.49
  208.4 2.5 %reshape_reshape.12 = bf16[512,1280]{1,0:T(8,128)(2,1)S(1)} reshape(bf16[64,2,4,1280]{3,2,1,0:T(4,128)(2,1)} %copy.49) | data formatting | bytes 2621440 | tf_op jit(solution)/shard_map/reshape;reshape | solution.py:25
  210.9 0.9 split.28
  211.8 0.8 split.29
  (35 shorter events, 2.5 us)
Async XLA Ops:
  0.6 22.8 %copy-start = (bf16[768,768]{1,0:T(8,128)(2,1)S(1)}, bf16[768,768]{1,0:T(8,128)(2,1)}, u32[]{:S(2)}) copy-start(bf16[768,768]{1,0:T(8,128)(2,1)} %param.13) | copy-start | bytes 3538948
  2.2 38.6 %all-to-all-start = ((bf16[64,4,512]{2,1,0:T(4,128)(2,1)}), bf16[64,4,512]{2,1,0:T(4,128)(2,1)S(1)}, u32[]{:S(2)}, u32[]{:S(2)}) async-start(bf16[64,4,512]{2,1,0:T(4,128)(2,1)} %broadcast_in_dim.24), calls=%async_computation | async-start | bytes 524288 | tf_op jit(solution)/shard_map/all_to_all | solution.py:19
  21.3 2.1 copy-start.7
  57.1 62.9 %copy-start.1 = (f32[2,768]{1,0:T(2,128)S(1)}, f32[2,768]{1,0:T(2,128)}, u32[]{:S(2)}) copy-start(f32[2,768]{1,0:T(2,128)} %param.17) | copy-start | bytes 18436
  57.1 62.9 %copy-start.2 = (f32[2,768]{1,0:T(2,128)S(1)}, f32[2,768]{1,0:T(2,128)}, u32[]{:S(2)}) copy-start(f32[2,768]{1,0:T(2,128)} %param.16) | copy-start | bytes 18436
  57.1 63.6 %copy-start.3 = (f32[2,512]{1,0:T(2,128)S(1)}, f32[2,512]{1,0:T(2,128)}, u32[]{:S(2)}) copy-start(f32[2,512]{1,0:T(2,128)} %param.23) | copy-start | bytes 12292
  57.1 63.6 %copy-start.4 = (f32[2,512]{1,0:T(2,128)S(1)}, f32[2,512]{1,0:T(2,128)}, u32[]{:S(2)}) copy-start(f32[2,512]{1,0:T(2,128)} %param.22) | copy-start | bytes 12292
  155.7 0.7 copy-start.5
  155.7 0.7 copy-start.8
  155.7 1.5 copy-start.6
  155.7 1.5 copy-start.9
where the time goes:
time: 213 us
  blocking collectives  152 us (71%)
  starting transfers between devices  19.1 us (9%)
  waiting for transfers between devices  15.4 us (7%)
  local copies, waits for them, and re-layouts  10.3 us (5%)
  matrix products  8.57 us (4%)
  other arithmetic  5.93 us (3%)
    all_to_all x7, blocking collectives, from_everyone(): return lax.all_to_all(copies, axis, split_axis=0, concat_axis=0, tiled=True)  120 us
    all_to_all x1, blocking collectives, sum_in_two_steps(): lax.all_to_all(own.astype(jnp.bfloat16), far, 0, 0, tiled=True)  27.2 us
    all_to_all x1, starting transfers between devices, from_everyone(): return lax.all_to_all(copies, axis, split_axis=0, concat_axis=0, tiled=True)  19.1 us
    all_to_all x1, waiting for transfers between devices, from_everyone(): return lax.all_to_all(copies, axis, split_axis=0, concat_axis=0, tiled=True)  15.4 us
  transfers between devices with their start and end apart: 1, of which 1 were waited for; matrix products, arithmetic and copies ran while one was open for 2% of the time, Pallas kernels for 0%

commit v1 on v0

v1 whole, which is shorter than its diff:
```python
import functools

import jax
import jax.numpy as jnp
from jax import lax
from jax.experimental import pallas as pl
from jax.experimental.pallas import tpu as pltpu
from jax.sharding import Mesh
from jax.sharding import PartitionSpec as P

AXES = ("z", "x", "c", "t")
FS = ("z", "x", "c")
MESH = pl.DeviceIdType.MESH
f32 = jnp.float32
bf16 = jnp.bfloat16

first_decay = 0.8
second_decay = 0.9
step_size = 0.5
mean_guard = 1e-06
root_guard = 1e-08


def log2(n):
    return n.bit_length() - 1


def part(v, low, size):
    return lax.shift_right_logical(v, low) & (size - 1)


def moved(rows, sizes):
    nz, nx, nc = sizes
    n = nz * nx * nc * rows
    lr, lz, lx, lc = log2(rows), log2(nz), log2(nx), log2(nc)
    nat = lax.broadcasted_iota(jnp.int32, (n, n), 0)
    got = lax.broadcasted_iota(jnp.int32, (n, n), 1)
    r = part(got, 0, rows)
    z = part(got, lr, nz)
    x = part(got, lr + lz, nx)
    c = part(got, lr + lz + lx, nc)
    want = ((z * nx + x) * nc + c) * rows + r
    return jnp.where(nat == want, 1.0, 0.0).astype(bf16)


def mul(a, b):
    return jnp.dot(a, b, preferred_element_type=f32)


def mul_t(a, b):
    return lax.dot_general(a, b, (((0,), (0,)), ((), ())), preferred_element_type=f32)


def kernel(sizes, widths, count, *refs):
    nz, nx, nc, nt = sizes
    qw, kw = widths
    (
        ql, qg, qm, qb, qf, qs, kl, kg, km, kb, kf, ks,
        qf_out, qs_out, qstep_out, qcopy_out, kf_out, ks_out, kstep_out, kcopy_out,
        ql_v, qg_v, kl_v, kg_v,
        bz, mo, mz, bslab, mslab, tokens, bnat, bperm, mnat, bwide, mwide, mold,
        prf, prs, rc, xs, rx, zf, zs, rz, ag, agf, sp, sz, hs,
        load_sem, zsend, zrecv, psend, precv, xsend, xrecv, csend, crecv,
    ) = refs
    w = qw + kw
    rank = qb.shape[1]
    z, x, c, t = (lax.axis_index(a) for a in AXES)
    other = 1 - c

    loads = [
        pltpu.make_async_copy(src, dst, load_sem.at[k])
        for k, (src, dst) in enumerate(((ql, ql_v), (qg, qg_v), (kl, kl_v), (kg, kg_v)))
    ]
    for load in loads:
        load.start()

    barrier = pltpu.get_barrier_semaphore()
    plane = nx * nc * nt
    mine = (x * nc + c) * nt + t

    def far(i):
        h = (i + 1) // 2
        return lax.rem(z + nz // 2 + h * (2 * lax.rem(i, 2) - 1) + nz, nz)

    def plane_peer(i):
        p = lax.rem(mine + i, plane)
        return (z, p // (nc * nt), lax.rem(p // nt, nc), lax.rem(p, nt)), p

    @pl.loop(0, nz - 1)
    def _(i):
        pl.semaphore_signal(barrier, inc=1, device_id=(far(i), x, c, t), device_id_type=MESH)

    @pl.loop(1, plane)
    def _(i):
        pl.semaphore_signal(barrier, inc=1, device_id=plane_peer(i)[0], device_id_type=MESH)

    bz[z, :, :rank] = qb[...]
    bz[z, :, rank:] = kb[...]
    mo[z, 0:2, :qw] = qf[...].astype(bf16)
    mo[z, 0:2, qw:] = kf[...].astype(bf16)
    mo[z, 2:4, :qw] = qs[...].astype(bf16)
    mo[z, 2:4, qw:] = ks[...].astype(bf16)
    mz[z, :, :qw] = qm[...].astype(bf16)
    mz[z, :, qw:] = km[...].astype(bf16)
    pl.semaphore_wait(barrier, nz - 1 + plane - 1)

    def z_copy(stage, src, dst, peer, slot):
        return pltpu.make_async_remote_copy(
            src_ref=src, dst_ref=dst,
            send_sem=zsend.at[stage, peer], recv_sem=zrecv.at[stage, slot],
            device_id=(peer, x, c, t), device_id_type=MESH,
        )

    def z_spread(stage, buf):
        @pl.loop(0, nz - 1)
        def _(i):
            z_copy(stage, buf.at[z], buf.at[z], far(i), z).start()

    def z_arrived(stage, buf):
        @pl.loop(0, nz - 1)
        def _(i):
            p = far(i)
            z_copy(stage, buf.at[p], buf.at[p], p, p).wait_recv()

    def z_left(stage, buf):
        @pl.loop(0, nz - 1)
        def _(i):
            p = far(i)
            z_copy(stage, buf.at[p], buf.at[p], p, p).wait_send()

    def x_copy(stage, src, dst, dx):
        p = lax.rem(x + dx, nx)
        return pltpu.make_async_remote_copy(
            src_ref=src, dst_ref=dst,
            send_sem=xsend.at[stage, dx], recv_sem=xrecv.at[stage, nx - dx],
            device_id=(z, p, c, t), device_id_type=MESH,
        )

    def x_from(stage, buf, dx):
        pltpu.make_async_remote_copy(
            src_ref=buf, dst_ref=buf,
            send_sem=xsend.at[stage, dx], recv_sem=xrecv.at[stage, dx],
            device_id=(z, lax.rem(x + dx, nx), c, t), device_id_type=MESH,
        ).wait_recv()

    def c_copy(stage, k, src, dst):
        return pltpu.make_async_remote_copy(
            src_ref=src, dst_ref=dst,
            send_sem=csend.at[stage, k], recv_sem=crecv.at[stage, k],
            device_id=(z, x, other, t), device_id_type=MESH,
        )

    def x_spread(stage, slabs):
        for dx in X_ORDER[nx]:
            x_copy(stage, slabs.at[c, x], slabs.at[c, x], dx).start()
        c_copy(stage, 0, slabs.at[c, x], slabs.at[c, x]).start()

    def x_onward(stage, slabs):
        for dx in X_ORDER[nx][::-1]:
            p = lax.rem(x + dx, nx)
            x_from(stage, slabs.at[c, p], dx)
            c_copy(stage, dx, slabs.at[c, p], slabs.at[c, p]).start()

    def x_arrived(stage, slabs):
        for dx in range(nx):
            p = lax.rem(x + dx, nx)
            c_copy(stage, dx, slabs.at[other, p], slabs.at[other, p]).wait_recv()

    def x_left(stage, slabs):
        for dx in range(1, nx):
            x_copy(stage, slabs.at[c, x], slabs.at[c, x], dx).wait_send()
        for dx in range(nx):
            p = lax.rem(x + dx, nx)
            c_copy(stage, dx, slabs.at[c, p], slabs.at[c, p]).wait_send()

    z_spread(0, bz)
    z_spread(1, mo)
    z_spread(2, mz)

    for load in loads[:2]:
        load.wait()
    tokens[:, :qw] = mul_t(ql_v[...], qg_v[...])
    for load in loads[2:]:
        load.wait()
    tokens[:, qw:] = mul_t(kl_v[...], kg_v[...])

    z_arrived(0, bz)
    lr = bz.shape[1]
    for k in range(nz):
        bwide[lr * k : lr * (k + 1), :] = bz[k].astype(f32)
    bslab[c, x] = bwide[...].astype(bf16)
    x_spread(0, bslab)
    by_latent = moved(lr, (nz, nx, nc))
    by_rank = moved(2, (nz, nx, nc))
    x_onward(0, bslab)
    x_arrived(0, bslab)
    latent = by_latent.shape[0]
    bnat[...] = mul(by_latent, bslab[...].reshape(latent, 2 * rank)).astype(bf16)
    bperm[:, :rank] = mul(bnat[:, :rank], by_rank).astype(bf16)
    bperm[:, rank:] = mul(bnat[:, rank:], by_rank).astype(bf16)

    def project(columns, basis):
        s = tokens[:, columns]
        high = s.astype(bf16)
        low = (s - high.astype(f32)).astype(bf16)
        got = mul_t(basis, high) + mul_t(basis, low)
        got = got.reshape(nc, nx, rank // (nc * nx), got.shape[1])
        prf[:, :, :, columns] = got
        prs[:, :, :, columns] = got.astype(bf16)

    project(slice(0, qw), bperm[:, :rank])
    project(slice(qw, w), bperm[:, rank:])

    order = X_ORDER[nx] + (0,)
    for dx in order:
        p = lax.rem(x + dx, nx)
        c_copy(1, dx, prs.at[other, p], rc.at[p]).start()
    for dx in order:
        p = lax.rem(x + dx, nx)
        c_copy(1, dx, rc.at[p], rc.at[p]).wait_recv()
        both = prf[c, p] + rc[p].astype(f32)
        if dx:
            xs[p] = both.astype(bf16)
            x_copy(1, xs.at[p], rx.at[x], dx).start()
        else:
            total = both

    z_arrived(2, mz)
    for k in range(nz):
        mwide[lr * k : lr * (k + 1), :] = mz[k].astype(f32)
    mslab[c, x] = mwide[...].astype(bf16)
    z_arrived(1, mo)
    for k in range(nz):
        mold[0, 2 * k : 2 * k + 2, :] = mo[k, 0:2].astype(f32)
        mold[1, 2 * k : 2 * k + 2, :] = mo[k, 2:4].astype(f32)
    x_spread(2, mslab)

    for dx in range(1, nx):
        p = lax.rem(x + dx, nx)
        x_from(1, rx.at[p], dx)
        total = total + rx[p].astype(f32)
    for k in range(nz):
        zf[k] = total[2 * k : 2 * k + 2]
        zs[k] = total[2 * k : 2 * k + 2].astype(bf16)
    rz[z] = jnp.zeros_like(rz[0])

    @pl.loop(0, nz - 1)
    def _(i):
        p = far(i)
        z_copy(3, zs.at[p], rz.at[z], p, z).start()

    x_onward(2, mslab)
    x_arrived(2, mslab)
    mnat[...] = mul(by_latent, mslab[...].reshape(latent, w))

    z_arrived(3, rz)
    proj = zf[z]
    for k in range(nz):
        proj = proj + rz[k].astype(f32)

    ag[z] = proj.astype(bf16)
    square = jnp.sum(proj * proj)
    sp[mine] = jnp.full((1, 128), square, f32)
    z_spread(4, ag)

    def p_copy(src, dst, peer, there, here):
        return pltpu.make_async_remote_copy(
            src_ref=src, dst_ref=dst,
            send_sem=psend.at[there], recv_sem=precv.at[here],
            device_id=peer, device_id_type=MESH,
        )

    @pl.loop(1, plane)
    def _(i):
        peer, p = plane_peer(i)
        p_copy(sp.at[mine], sp.at[mine], peer, p, mine).start()

    @pl.loop(1, plane)
    def _(i):
        peer, p = plane_peer(i)
        p_copy(sp.at[p], sp.at[p], peer, p, p).wait_recv()

    sz[z] = jnp.sum(sp[...], axis=0)
    z_spread(5, sz)
    z_arrived(4, ag)
    for k in range(nz):
        agf[2 * k : 2 * k + 2, :] = ag[k].astype(f32)
    z_arrived(5, sz)
    mean = jnp.sum(sz[...], axis=0)[:, 0:1] / count + mean_guard
    root_mean = jnp.sqrt(mean)

    def moments(scaled, first_old, second_old):
        first = first_decay * first_old + (1.0 - first_decay) * scaled
        second = second_decay * second_old + (1.0 - second_decay) * scaled * scaled
        return first, second

    first, second = moments(agf[...] / root_mean, mold[0], mold[1])
    hs[c, x] = (first / (jnp.sqrt(second) + root_guard)).astype(bf16)
    x_spread(3, hs)

    scaled = proj / root_mean
    first, second = moments(scaled[:, :qw], qf[...], qs[...])
    qf_out[...] = first
    qs_out[...] = second
    first, second = moments(scaled[:, qw:], kf[...], ks[...])
    kf_out[...] = first
    ks_out[...] = second
    own_q = mul(qb[...], by_rank).astype(bf16)
    own_k = mul(kb[...], by_rank).astype(bf16)

    x_onward(3, hs)
    x_arrived(3, hs)
    heading = hs[...].reshape(rank, w)
    qcopy_out[...] = (mnat[:, :qw] - step_size * mul(bperm[:, :rank], heading[:, :qw])).astype(bf16)
    kcopy_out[...] = (mnat[:, qw:] - step_size * mul(bperm[:, rank:], heading[:, qw:])).astype(bf16)
    qstep_out[...] = mul(own_q, heading[:, :qw])
    kstep_out[...] = mul(own_k, heading[:, qw:])

    for stage, buf in enumerate((bz, mo, mz, rz, ag, sz)):
        z_left(stage, buf)

    @pl.loop(1, plane)
    def _(i):
        peer, p = plane_peer(i)
        p_copy(sp.at[p], sp.at[p], peer, p, p).wait_send()

    x_left(0, bslab)
    x_left(2, mslab)
    x_left(3, hs)
    for dx in range(1, nx):
        p = lax.rem(x + dx, nx)
        x_copy(1, xs.at[p], rx.at[x], dx).wait_send()
    for dx in range(nx):
        p = lax.rem(x + dx, nx)
        c_copy(1, dx, prs.at[other, p], rc.at[p]).wait_send()


X_ORDER = {2: (1,), 4: (2, 1, 3)}


def body(sizes, *args):
    nz, nx, nc, nt = sizes
    ql, qg, qm, qb, qf, qs, kl, kg, km, kb, kf, ks = args
    qw, kw = qg.shape[1], kg.shape[1]
    w = qw + kw
    fs = nz * nx * nc
    lr, rank = qb.shape
    latent = lr * fs
    rows = rank // (nc * nx)
    count = float(rank * w * nt)
    plane = nx * nc * nt
    vmem = pl.BlockSpec(memory_space=pltpu.VMEM)
    anywhere = pl.BlockSpec(memory_space=pl.ANY)
    shape = jax.ShapeDtypeStruct
    return pl.pallas_call(
        functools.partial(kernel, sizes, (qw, kw), count),
        out_shape=(
            shape(qf.shape, f32), shape(qs.shape, f32), shape(qm.shape, f32), shape((latent, qw), bf16),
            shape(kf.shape, f32), shape(ks.shape, f32), shape(km.shape, f32), shape((latent, kw), bf16),
        ),
        in_specs=[anywhere, anywhere, vmem, vmem, vmem, vmem] * 2,
        out_specs=[vmem] * 8,
        scratch_shapes=[
            pltpu.VMEM(ql.shape, bf16), pltpu.VMEM(qg.shape, bf16),
            pltpu.VMEM(kl.shape, bf16), pltpu.VMEM(kg.shape, bf16),
            pltpu.VMEM((nz, lr, 2 * rank), bf16),
            pltpu.VMEM((nz, 4, w), bf16),
            pltpu.VMEM((nz, lr, w), bf16),
            pltpu.VMEM((nc, nx, nz * lr, 2 * rank), bf16),
            pltpu.VMEM((nc, nx, nz * lr, w), bf16),
            pltpu.VMEM((latent, w), f32),
            pltpu.VMEM((latent, 2 * rank), bf16),
            pltpu.VMEM((latent, 2 * rank), bf16),
            pltpu.VMEM((latent, w), f32),
            pltpu.VMEM((nz * lr, 2 * rank), f32),
            pltpu.VMEM((nz * lr, w), f32),
            pltpu.VMEM((2, rows, w), f32),
            pltpu.VMEM((nc, nx, rows, w), f32),
            pltpu.VMEM((nc, nx, rows, w), bf16),
            pltpu.VMEM((nx, rows, w), bf16),
            pltpu.VMEM((nx, rows, w), bf16),
            pltpu.VMEM((nx, rows, w), bf16),
            pltpu.VMEM((nz, 2, w), f32),
            pltpu.VMEM((nz, 2, w), bf16),
            pltpu.VMEM((nz, 2, w), bf16),
            pltpu.VMEM((nz, 2, w), bf16),
            pltpu.VMEM((rows, w), f32),
            pltpu.VMEM((plane, 1, 128), f32),
            pltpu.VMEM((nz, 1, 128), f32),
            pltpu.VMEM((nc, nx, rows, w), bf16),
            pltpu.SemaphoreType.DMA((4,)),
            pltpu.SemaphoreType.DMA((6, nz)), pltpu.SemaphoreType.DMA((6, nz)),
            pltpu.SemaphoreType.DMA((plane,)), pltpu.SemaphoreType.DMA((plane,)),
            pltpu.SemaphoreType.DMA((4, nx)), pltpu.SemaphoreType.DMA((4, nx)),
            pltpu.SemaphoreType.DMA((4, nx)), pltpu.SemaphoreType.DMA((4, nx)),
        ],
        compiler_params=pltpu.CompilerParams(
            collective_id=0, has_side_effects=True, vmem_limit_bytes=56 * 1024 * 1024
        ),
    )(*args)


def solution(mesh, chips=(16, 4, 2)):
    nt = mesh.shape["tp"]
    finer = Mesh(mesh.devices.reshape(*chips, nt), AXES)
    in_specs = (P(FS, None), P(FS, "t"), P(FS, "t"), P(FS, None), P(FS, "t"), P(FS, "t")) * 2
    out_specs = (P(FS, "t"), P(FS, "t"), P(FS, "t"), P(None, "t")) * 2
    return jax.shard_map(
        functools.partial(body, (*chips, nt)), mesh=finer, in_specs=in_specs, out_specs=out_specs, check_vma=False
    )
```

time: 213 us -> 85.5 us (0.40)
  blocking collectives: 152 us -> 0 us
  Pallas kernels: 0 us -> 75.9 us
  starting transfers between devices: 19.1 us -> 0 us
  waiting for transfers between devices: 15.4 us -> 0 us
  matrix products: 8.57 us -> 0 us
  other arithmetic: 5.93 us -> 0 us
    all_to_all x9 -> x0, blocking collectives: 152 us -> none  [the longest x7 120 us: from_everyone(): return lax.all_to_all(copies, axis, split_axis=0, concat_axis=0, tiled=True)]
    pallas_call x0 -> x1, Pallas kernels: none -> 75.9 us  [body(): pl.pallas_call(functools.partial(kernel, sizes, (qw, kw), count), out_sha...]
    all_to_all x1 -> x0, starting transfers between devices: 19.1 us -> none  [from_everyone(): return lax.all_to_all(copies, axis, split_axis=0, concat_axis=0, tiled=True)]
    all_to_all x1 -> x0, waiting for transfers between devices: 15.4 us -> none  [from_everyone(): return lax.all_to_all(copies, axis, split_axis=0, concat_axis=0, tiled=True)]
    dot_general x6 -> x0, matrix products: 8.57 us -> none  [the longest x2 4.01 us: across_tokens(): lax.dot_general(left, right, (((0,), (0,)), ((), ())), preferred_element_...]
    unnamed x20 -> x16, local copies, waits for them, and re-layouts: 0.05 us -> 8.59 us
    reduce_sum x5 -> x0, other arithmetic: 3.33 us -> none  [the longest x1 1.38 us: sum_at_owner(): return arrived.astype(jnp.float32).sum(axis=0)]
    broadcast_in_dim x8 -> x0, local copies, waits for them, and re-layouts: 3.25 us -> none  [from_everyone(): copies = jnp.broadcast_to(x, (lax.axis_size(axis), *x.shape))]
  transfers between devices with their start and end apart: 1 -> 0, of which waited for: 1 -> 0; matrix products, arithmetic and copies ran while one was open for 2% -> 0% of each run, Pallas kernels for 0% -> 0%
where the time goes in v1:
time: 85.5 us; the launch traced here: 85.2 us
  Pallas kernels  75.9 us (89%)
  local copies, waits for them, and re-layouts  8.59 us (10%)
    pallas_call x1, Pallas kernels, body(): pl.pallas_call(functools.partial(kernel, sizes, (qw, kw), count), out_sha...  75.9 us
    unnamed x16, local copies, waits for them, and re-layouts  8.59 us

profile of v1, /device:TPU:1, one launch (start us, length us, event | category | flops | bytes accessed | tf_op | source)
XLA Modules:
  0.0 85.2 jit_solution(11429934139051748641)
XLA Ops:
  0.6 75.9 %shard_map.179 = (f32[2,768]{1,0:T(2,128)}, f32[2,768]{1,0:T(2,128)}, f32[4,768]{1,0:T(4,128)}, bf16[512,768]{1,0:T(8,128)(2,1)}, f32[2,512]{1,0:T(2,128)}, /*in...) custom-call(bf16[768,512]{1,0:T(8,128)(2,1)} %refs_0_.1, bf16[768,768]{1,0:T(8,128)(2,1)} %refs_1_.1, ...), custom_call_target="tpu_custom_call" | custom-call | tf_op jit(solution)/shard_map/pallas_call | solution.py:355
  76.6 0.0 copy-start.3
  76.6 0.0 copy-start.2
  76.6 0.0 copy-start.1
  76.6 0.0 copy-start
  76.6 1.3 %copy.28 = f32[2,768]{1,0:T(2,128)} copy(f32[2,768]{1,0:T(2,128)} %get-tuple-element.16) | data formatting | bytes 12288
  78.0 1.3 %copy.29 = f32[2,768]{1,0:T(2,128)} copy(f32[2,768]{1,0:T(2,128)} %get-tuple-element.17) | data formatting | bytes 12288
  79.2 1.3 %copy.30 = f32[4,768]{1,0:T(4,128)} copy(f32[4,768]{1,0:T(4,128)} %get-tuple-element.18) | data formatting | bytes 24576
  80.5 2.1 %copy.31 = bf16[512,768]{1,0:T(8,128)(2,1)} copy(bf16[512,768]{1,0:T(8,128)(2,1)} %get-tuple-element.19) | data formatting | bytes 1572864
  82.6 0.0 copy-done.3
  82.6 0.6 copy.32
  83.2 0.0 copy-done.2
  83.2 0.6 copy.33
  83.8 0.0 copy-done.1
  83.8 0.6 copy.34
  84.4 0.0 copy-done
  84.4 0.8 copy.35
Async XLA Ops:
  76.6 6.0 %copy-start.3 = (f32[2,512]{1,0:T(2,128)S(1)}, f32[2,512]{1,0:T(2,128)}, u32[]{:S(2)}) copy-start(f32[2,512]{1,0:T(2,128)} %get-tuple-element.20) | copy-start | bytes 12292
  76.6 6.6 %copy-start.2 = (f32[2,512]{1,0:T(2,128)S(1)}, f32[2,512]{1,0:T(2,128)}, u32[]{:S(2)}) copy-start(f32[2,512]{1,0:T(2,128)} %get-tuple-element.21) | copy-start | bytes 12292
  76.6 7.2 %copy-start.1 = (f32[4,512]{1,0:T(4,128)S(1)}, f32[4,512]{1,0:T(4,128)}, u32[]{:S(2)}) copy-start(f32[4,512]{1,0:T(4,128)} %get-tuple-element.22) | copy-start | bytes 24580
  76.6 7.8 %copy-start = (bf16[512,512]{1,0:T(8,128)(2,1)S(1)}, bf16[512,512]{1,0:T(8,128)(2,1)}, u32[]{:S(2)}) copy-start(bf16[512,512]{1,0:T(8,128)(2,1)} %get-tuple-element.23) | copy-start | bytes 1572868

commit v2 on v1

--- a/solution.py
+++ b/solution.py
@@ -55,11 +55,11 @@
     nz, nx, nc, nt = sizes
     qw, kw = widths
     (
-        ql, qg, qm, qb, qf, qs, kl, kg, km, kb, kf, ks,
-        qf_out, qs_out, qstep_out, qcopy_out, kf_out, ks_out, kstep_out, kcopy_out,
-        ql_v, qg_v, kl_v, kg_v,
-        bz, mo, mz, bslab, mslab, tokens, bnat, bperm, mnat, bwide, mwide, mold,
-        prf, prs, rc, xs, rx, zf, zs, rz, ag, agf, sp, sz, hs,
+        ql, qg, qm_h, qb, qf_h, qs_h, kl, kg, km_h, kb, kf_h, ks_h,
+        hs, bperm, mnat, proj_out, mean_out,
+        ql_v, qg_v, kl_v, kg_v, qm, qf, qs, km, kf, ks,
+        bz, mo, mz, bslab, mslab, tokens, bnat, bwide, mwide, mold,
+        prf, prs, rc, xs, rx, zf, zs, rz, ag, agf, sp, sz,
         load_sem, zsend, zrecv, psend, precv, xsend, xrecv, csend, crecv,
     ) = refs
     w = qw + kw
@@ -69,9 +69,13 @@
 
     loads = [
         pltpu.make_async_copy(src, dst, load_sem.at[k])
-        for k, (src, dst) in enumerate(((ql, ql_v), (qg, qg_v), (kl, kl_v), (kg, kg_v)))
+        for k, (src, dst) in enumerate((
+            (ql, ql_v), (qg, qg_v), (kl, kl_v), (kg, kg_v),
+            (qb, bz.at[z, :, :rank]), (kb, bz.at[z, :, rank:]),
+            (qf_h, qf), (qs_h, qs), (kf_h, kf), (ks_h, ks), (qm_h, qm), (km_h, km),
+        ))
     ]
-    for load in loads:
+    for load in loads[4:] + loads[:4]:
         load.start()
 
     barrier = pltpu.get_barrier_semaphore()
@@ -94,8 +98,8 @@
     def _(i):
         pl.semaphore_signal(barrier, inc=1, device_id=plane_peer(i)[0], device_id_type=MESH)
 
-    bz[z, :, :rank] = qb[...]
-    bz[z, :, rank:] = kb[...]
+    for load in loads[4:]:
+        load.wait()
     mo[z, 0:2, :qw] = qf[...].astype(bf16)
     mo[z, 0:2, qw:] = kf[...].astype(bf16)
     mo[z, 2:4, :qw] = qs[...].astype(bf16)
@@ -180,7 +184,7 @@
     for load in loads[:2]:
         load.wait()
     tokens[:, :qw] = mul_t(ql_v[...], qg_v[...])
-    for load in loads[2:]:
+    for load in loads[2:4]:
         load.wait()
     tokens[:, qw:] = mul_t(kl_v[...], kg_v[...])
 
@@ -251,7 +255,7 @@
 
     x_onward(2, mslab)
     x_arrived(2, mslab)
-    mnat[...] = mul(by_latent, mslab[...].reshape(latent, w))
+    mnat[...] = mul(by_latent, mslab[...].reshape(latent, w)).astype(bf16)
 
     z_arrived(3, rz)
     proj = zf[z]
@@ -289,33 +293,14 @@
     mean = jnp.sum(sz[...], axis=0)[:, 0:1] / count + mean_guard
     root_mean = jnp.sqrt(mean)
 
-    def moments(scaled, first_old, second_old):
-        first = first_decay * first_old + (1.0 - first_decay) * scaled
-        second = second_decay * second_old + (1.0 - second_decay) * scaled * scaled
-        return first, second
-
     first, second = moments(agf[...] / root_mean, mold[0], mold[1])
     hs[c, x] = (first / (jnp.sqrt(second) + root_guard)).astype(bf16)
     x_spread(3, hs)
 
-    scaled = proj / root_mean
-    first, second = moments(scaled[:, :qw], qf[...], qs[...])
-    qf_out[...] = first
-    qs_out[...] = second
-    first, second = moments(scaled[:, qw:], kf[...], ks[...])
-    kf_out[...] = first
-    ks_out[...] = second
-    own_q = mul(qb[...], by_rank).astype(bf16)
-    own_k = mul(kb[...], by_rank).astype(bf16)
-
+    proj_out[...] = proj
+    mean_out[...] = jnp.broadcast_to(root_mean, mean_out.shape)
     x_onward(3, hs)
     x_arrived(3, hs)
-    heading = hs[...].reshape(rank, w)
-    qcopy_out[...] = (mnat[:, :qw] - step_size * mul(bperm[:, :rank], heading[:, :qw])).astype(bf16)
-    kcopy_out[...] = (mnat[:, qw:] - step_size * mul(bperm[:, rank:], heading[:, qw:])).astype(bf16)
-    qstep_out[...] = mul(own_q, heading[:, :qw])
-    kstep_out[...] = mul(own_k, heading[:, qw:])
-
     for stage, buf in enumerate((bz, mo, mz, rz, ag, sz)):
         z_left(stage, buf)
 
@@ -335,11 +320,42 @@
         c_copy(1, dx, prs.at[other, p], rc.at[p]).wait_send()
 
 
+def moments(scaled, first_old, second_old):
+    first = first_decay * first_old + (1.0 - first_decay) * scaled
+    second = second_decay * second_old + (1.0 - second_decay) * scaled * scaled
+    return first, second
+
+
+def finish(sizes, *refs):
+    (
+        heading, basis, master, proj, mean, qb, qf, qs, kb, kf, ks,
+        qf_out, qs_out, qstep_out, qcopy_out, kf_out, ks_out, kstep_out, kcopy_out,
+    ) = refs
+    nz, nx, nc, nt = sizes
+    rank = qb.shape[1]
+    qw = qf.shape[1]
+    by_rank = moved(2, (nz, nx, nc))
+    scaled = proj[...] / mean[:, 0:1]
+    qf_out[...], qs_out[...] = moments(scaled[:, :qw], qf[...], qs[...])
+    kf_out[...], ks_out[...] = moments(scaled[:, qw:], kf[...], ks[...])
+    own_q = mul(qb[...], by_rank).astype(bf16)
+    own_k = mul(kb[...], by_rank).astype(bf16)
+    q_dir = heading[:, :qw]
+    k_dir = heading[:, qw:]
+    qstep_out[...] = mul(own_q, q_dir)
+    kstep_out[...] = mul(own_k, k_dir)
+    q_step = mul(basis[:, :rank], q_dir)
+    qcopy_out[...] = (master[:, :qw].astype(f32) - step_size * q_step).astype(bf16)
+    k_step = mul(basis[:, rank:], k_dir)
+    kcopy_out[...] = (master[:, qw:].astype(f32) - step_size * k_step).astype(bf16)
+
+
 X_ORDER = {2: (1,), 4: (2, 1, 3)}
 
 
 def body(sizes, *args):
     nz, nx, nc, nt = sizes
+    args = [pltpu.with_memory_space_constraint(a, pltpu.HBM) for a in args]
     ql, qg, qm, qb, qf, qs, kl, kg, km, kb, kf, ks = args
     qw, kw = qg.shape[1], kg.shape[1]
     w = qw + kw
@@ -350,19 +366,20 @@
     count = float(rank * w * nt)
     plane = nx * nc * nt
     vmem = pl.BlockSpec(memory_space=pltpu.VMEM)
-    anywhere = pl.BlockSpec(memory_space=pl.ANY)
     shape = jax.ShapeDtypeStruct
-    return pl.pallas_call(
+    hbm = pl.BlockSpec(memory_space=pltpu.HBM)
+    heading, basis, master, proj, mean = pl.pallas_call(
         functools.partial(kernel, sizes, (qw, kw), count),
         out_shape=(
-            shape(qf.shape, f32), shape(qs.shape, f32), shape(qm.shape, f32), shape((latent, qw), bf16),
-            shape(kf.shape, f32), shape(ks.shape, f32), shape(km.shape, f32), shape((latent, kw), bf16),
+            shape((nc, nx, rows, w), bf16), shape((latent, 2 * rank), bf16), shape((latent, w), bf16),
+            shape((2, w), f32), shape((1, 128), f32),
         ),
-        in_specs=[anywhere, anywhere, vmem, vmem, vmem, vmem] * 2,
-        out_specs=[vmem] * 8,
+        in_specs=[hbm] * 12,
+        out_specs=[vmem] * 5,
         scratch_shapes=[
             pltpu.VMEM(ql.shape, bf16), pltpu.VMEM(qg.shape, bf16),
             pltpu.VMEM(kl.shape, bf16), pltpu.VMEM(kg.shape, bf16),
+            *(pltpu.VMEM(a.shape, f32) for a in (qm, qf, qs, km, kf, ks)),
             pltpu.VMEM((nz, lr, 2 * rank), bf16),
             pltpu.VMEM((nz, 4, w), bf16),
             pltpu.VMEM((nz, lr, w), bf16),
@@ -370,8 +387,6 @@
             pltpu.VMEM((nc, nx, nz * lr, w), bf16),
             pltpu.VMEM((latent, w), f32),
             pltpu.VMEM((latent, 2 * rank), bf16),
-            pltpu.VMEM((latent, 2 * rank), bf16),
-            pltpu.VMEM((latent, w), f32),
             pltpu.VMEM((nz * lr, 2 * rank), f32),
             pltpu.VMEM((nz * lr, w), f32),
             pltpu.VMEM((2, rows, w), f32),
@@ -387,17 +402,26 @@
             pltpu.VMEM((rows, w), f32),
             pltpu.VMEM((plane, 1, 128), f32),
             pltpu.VMEM((nz, 1, 128), f32),
-            pltpu.VMEM((nc, nx, rows, w), bf16),
-            pltpu.SemaphoreType.DMA((4,)),
+            pltpu.SemaphoreType.DMA((12,)),
             pltpu.SemaphoreType.DMA((6, nz)), pltpu.SemaphoreType.DMA((6, nz)),
             pltpu.SemaphoreType.DMA((plane,)), pltpu.SemaphoreType.DMA((plane,)),
             pltpu.SemaphoreType.DMA((4, nx)), pltpu.SemaphoreType.DMA((4, nx)),
             pltpu.SemaphoreType.DMA((4, nx)), pltpu.SemaphoreType.DMA((4, nx)),
         ],
         compiler_params=pltpu.CompilerParams(
-            collective_id=0, has_side_effects=True, vmem_limit_bytes=56 * 1024 * 1024
+            collective_id=0, has_side_effects=True, vmem_limit_bytes=28 * 1024 * 1024
         ),
     )(*args)
+    return pl.pallas_call(
+        functools.partial(finish, sizes),
+        out_shape=(
+            shape(qf.shape, f32), shape(qs.shape, f32), shape(qm.shape, f32), shape((latent, qw), bf16),
+            shape(kf.shape, f32), shape(ks.shape, f32), shape(km.shape, f32), shape((latent, kw), bf16),
+        ),
+        in_specs=[vmem] * 11,
+        out_specs=[vmem] * 8,
+        compiler_params=pltpu.CompilerParams(vmem_limit_bytes=20 * 1024 * 1024),
+    )(heading.reshape(rank, w), basis, master, proj, mean, qb, qf, qs, kb, kf, ks)
 
 
 def solution(mesh, chips=(16, 4, 2)):

time: 85.5 us -> 76.4 us (0.89)
  local copies, waits for them, and re-layouts: 8.59 us -> 0 us
    unnamed x16 -> x0, local copies, waits for them, and re-layouts: 8.59 us -> none
    pallas_call x1, Pallas kernels: 75.9 us -> 73.2 us  [body(): pl.pallas_call(functools.partial(kernel, sizes, (qw, kw), count), out_sha...]
    pallas_call x0 -> x1, Pallas kernels: none -> 2.44 us  [body(): pl.pallas_call(functools.partial(finish, sizes), out_shape=(shape(qf.shap...]
where the time goes in v2:
time: 76.4 us; the launch traced here: 76.3 us
  Pallas kernels  75.6 us (99%)
    pallas_call x1, Pallas kernels, body(): pl.pallas_call(functools.partial(kernel, sizes, (qw, kw), count), out_sha...  73.2 us
    pallas_call x1, Pallas kernels, body(): pl.pallas_call(functools.partial(finish, sizes), out_shape=(shape(qf.shap...  2.44 us

profile of v2, /device:TPU:1, one launch (start us, length us, event | category | flops | bytes accessed | tf_op | source)
XLA Modules:
  0.0 76.3 jit_solution(15681846742136998927)
XLA Ops:
  0.6 73.2 %shard_map.179 = (bf16[2,4,32,1280]{3,2,1,0:T(8,128)(2,1)S(1)}, bf16[512,512]{1,0:T(8,128)(2,1)S(1)}, bf16[512,1280]{1,0:T(8,128)(2,1)S(1)}, f32[2,1280]{1,0:T(2,128)S(1)}, f32[1,128]{1,0:T(1,128)S(1)}) custom-call(bf16[768,512]{1,0:T(8,128)(2,1)} %refs_0_.1, bf16[768,768]{1,0:T(8,128)(2,1)} %refs_1_.1, f32[4,768]{1,0:T(4,128)} %refs_2_.1, ...), custom_call_target="tpu_custom_call" | custom-call | tf_op jit(solution)/shard_map/pallas_call | solution.py:371
  73.8 2.4 %shard_map.180 = (f32[2,768]{1,0:T(2,128)}, f32[2,768]{1,0:T(2,128)}, f32[4,768]{1,0:T(4,128)}, bf16[512,768]{1,0:T(8,128)(2,1)}, f32[2,512]{1,0:T(2,128)}, /*in...) custom-call(bf16[256,1280]{1,0:T(8,128)(2,1)S(1)} %bitcast.1, ...), custom_call_target="tpu_custom_call" | custom-call | tf_op jit(solution)/shard_map/pallas_call | solution.py:415

commit v3 on v2

v3 whole, which is shorter than its diff:
```python
import functools

import jax
import jax.numpy as jnp
from jax import lax
from jax.experimental import pallas as pl
from jax.experimental.pallas import tpu as pltpu
from jax.sharding import Mesh
from jax.sharding import PartitionSpec as P

AXES = ("z", "x", "c", "t")
FS = ("z", "x", "c")
MESH = pl.DeviceIdType.MESH
f32 = jnp.float32
bf16 = jnp.bfloat16

first_decay = 0.8
second_decay = 0.9
step_size = 0.5
mean_guard = 1e-06
root_guard = 1e-08


def log2(n):
    return n.bit_length() - 1


def part(v, low, size):
    return lax.shift_right_logical(v, low) & (size - 1)


def moved(rows, sizes, back=False):
    nz, nx, nc = sizes
    n = nz * nx * nc * rows
    lr, lz, lx, lc = log2(rows), log2(nz), log2(nx), log2(nc)
    nat = lax.broadcasted_iota(jnp.int32, (n, n), int(back))
    got = lax.broadcasted_iota(jnp.int32, (n, n), 1 - int(back))
    r = part(got, 0, rows)
    z = part(got, lr, nz)
    x = part(got, lr + lz, nx)
    c = part(got, lr + lz + lx, nc)
    want = ((z * nx + x) * nc + c) * rows + r
    return jnp.where(nat == want, 1.0, 0.0).astype(bf16)


def mul(a, b):
    return jnp.dot(a, b, preferred_element_type=f32)


def mul_by_t(a, b):
    return lax.dot_general(a, b, (((1,), (1,)), ((), ())), preferred_element_type=f32)


def mul_t(a, b):
    return lax.dot_general(a, b, (((0,), (0,)), ((), ())), preferred_element_type=f32)


def kernel(sizes, widths, count, *refs):
    nz, nx, nc, nt = sizes
    qw, kw = widths
    (
        ql, qg, qm_h, qb, qf_h, qs_h, kl, kg, km_h, kb, kf_h, ks_h,
        heads, ps, bnat, mnat, scale_out,
        ql_v, qg_v, kl_v, kg_v, qm, qf, qs, km, kf, ks,
        bz, mo, mz, bslab, oslab, mslab, tokens, rounded, wide, wider, mold,
        rc, xs, rx, hilo, pt, zs, rz, ag, sp, sz,
        load_sem, zsend, zrecv, psend, precv, xsend, xrecv, csend, crecv,
    ) = refs
    w = qw + kw
    rank = qb.shape[1]
    lr = bz.shape[1]
    latent = lr * nz * nx * nc
    share = w // (nc * nx)
    lanes = pt.shape[2]
    halves = rank // lanes
    pairs = share // nz // 2
    z, x, c, t = (lax.axis_index(a) for a in AXES)
    other = 1 - c

    loads = [
        pltpu.make_async_copy(src, dst, load_sem.at[k])
        for k, (src, dst) in enumerate((
            (ql, ql_v), (qg, qg_v), (kl, kl_v), (kg, kg_v),
            (qb, bz.at[z, :, :rank]), (kb, bz.at[z, :, rank:]),
            (qf_h, qf), (qs_h, qs), (kf_h, kf), (ks_h, ks), (qm_h, qm), (km_h, km),
        ))
    ]
    for load in loads:
        load.start()

    barrier = pltpu.get_barrier_semaphore()
    plane = nx * nc * nt
    mine = (x * nc + c) * nt + t

    def far(i):
        h = (i + 1) // 2
        return lax.rem(z + nz // 2 + h * (2 * lax.rem(i, 2) - 1) + nz, nz)

    def plane_peer(i):
        p = lax.rem(mine + i, plane)
        return (z, p // (nc * nt), lax.rem(p // nt, nc), lax.rem(p, nt)), p

    @pl.loop(0, nz - 1)
    def _(i):
        pl.semaphore_signal(barrier, inc=1, device_id=(far(i), x, c, t), device_id_type=MESH)

    @pl.loop(1, plane)
    def _(i):
        pl.semaphore_signal(barrier, inc=1, device_id=plane_peer(i)[0], device_id_type=MESH)

    def z_copy(stage, src, dst, peer, slot):
        return pltpu.make_async_remote_copy(
            src_ref=src, dst_ref=dst,
            send_sem=zsend.at[stage, peer], recv_sem=zrecv.at[stage, slot],
            device_id=(peer, x, c, t), device_id_type=MESH,
        )

    def z_spread(stage, buf):
        @pl.loop(0, nz - 1)
        def _(i):
            z_copy(stage, buf.at[z], buf.at[z], far(i), z).start()

    def z_arrived(stage, buf):
        @pl.loop(0, nz - 1)
        def _(i):
            p = far(i)
            z_copy(stage, buf.at[p], buf.at[p], p, p).wait_recv()

    def z_left(stage, buf):
        @pl.loop(0, nz - 1)
        def _(i):
            p = far(i)
            z_copy(stage, buf.at[p], buf.at[p], p, p).wait_send()

    def x_copy(stage, src, dst, dx):
        p = lax.rem(x + dx, nx)
        return pltpu.make_async_remote_copy(
            src_ref=src, dst_ref=dst,
            send_sem=xsend.at[stage, dx], recv_sem=xrecv.at[stage, nx - dx],
            device_id=(z, p, c, t), device_id_type=MESH,
        )

    def x_from(stage, buf, dx):
        pltpu.make_async_remote_copy(
            src_ref=buf, dst_ref=buf,
            send_sem=xsend.at[stage, dx], recv_sem=xrecv.at[stage, dx],
            device_id=(z, lax.rem(x + dx, nx), c, t), device_id_type=MESH,
        ).wait_recv()

    def c_copy(stage, k, src, dst):
        return pltpu.make_async_remote_copy(
            src_ref=src, dst_ref=dst,
            send_sem=csend.at[stage, k], recv_sem=crecv.at[stage, k],
            device_id=(z, x, other, t), device_id_type=MESH,
        )

    def x_spread(stage, slabs):
        for dx in X_ORDER[nx]:
            x_copy(stage, slabs.at[c, x], slabs.at[c, x], dx).start()
        c_copy(stage, 0, slabs.at[c, x], slabs.at[c, x]).start()

    def x_onward(stage, slabs):
        for dx in X_ORDER[nx][::-1]:
            p = lax.rem(x + dx, nx)
            x_from(stage, slabs.at[c, p], dx)
            c_copy(stage, dx, slabs.at[c, p], slabs.at[c, p]).start()

    def x_arrived(stage, slabs):
        for dx in range(nx):
            p = lax.rem(x + dx, nx)
            c_copy(stage, dx, slabs.at[other, p], slabs.at[other, p]).wait_recv()

    def x_left(stage, slabs):
        for dx in range(1, nx):
            x_copy(stage, slabs.at[c, x], slabs.at[c, x], dx).wait_send()
        for dx in range(nx):
            p = lax.rem(x + dx, nx)
            c_copy(stage, dx, slabs.at[c, p], slabs.at[c, p]).wait_send()

    def rows(core, p):
        return pl.ds(pl.multiple_of((core * nx + p) * share, share), share)

    for load in loads[:2]:
        load.wait()
    tokens[:qw] = mul_t(qg_v[...], ql_v[...])
    for load in loads[2:4]:
        load.wait()
    tokens[qw:] = mul_t(kg_v[...], kl_v[...])
    rounded[...] = tokens[...].astype(bf16)
    for load in loads[4:]:
        load.wait()
    mo[z, 0:2, :qw] = qf[...].astype(bf16)
    mo[z, 0:2, qw:] = kf[...].astype(bf16)
    mo[z, 2:4, :qw] = qs[...].astype(bf16)
    mo[z, 2:4, qw:] = ks[...].astype(bf16)
    mz[z, :, :qw] = qm[...].astype(bf16)
    mz[z, :, qw:] = km[...].astype(bf16)
    pl.semaphore_wait(barrier, nz - 1 + plane - 1)

    order = X_ORDER[nx] + (0,)
    z_spread(0, bz)
    for dx in order:
        p = lax.rem(x + dx, nx)
        c_copy(1, dx, rounded.at[rows(other, p)], rc.at[p]).start()
    z_spread(1, mo)
    z_spread(2, mz)
    for dx in order:
        p = lax.rem(x + dx, nx)
        c_copy(1, dx, rc.at[p], rc.at[p]).wait_recv()
        both = tokens[rows(c, p)] + rc[p].astype(f32)
        if dx:
            xs[p] = both.astype(bf16)
            x_copy(1, xs.at[p], rx.at[x], dx).start()
        else:
            tokens[rows(c, p)] = both
    by_latent = moved(lr, (nz, nx, nc))

    z_arrived(0, bz)
    for k in range(nz):
        wide[lr * k : lr * (k + 1), :] = bz[k].astype(f32)
    bslab[c, x] = wide[...].astype(bf16)
    x_spread(0, bslab)

    total = tokens[rows(c, x)]
    for dx in range(1, nx):
        p = lax.rem(x + dx, nx)
        x_from(1, rx.at[p], dx)
        total = total + rx[p].astype(f32)
    high = total.astype(bf16)
    low = (total - high.astype(f32)).astype(bf16)
    part_of = latent // nc
    turned_high = mul(high, by_latent).astype(bf16)
    turned_low = mul(low, by_latent).astype(bf16)
    for k in range(nc):
        hilo[k, :share] = turned_high[:, k * part_of : (k + 1) * part_of]
        hilo[k, share:] = turned_low[:, k * part_of : (k + 1) * part_of]

    x_onward(0, bslab)
    got = mul(hilo[c], bslab[c].reshape(part_of, 2 * rank))
    x_arrived(0, bslab)
    got = got + mul(hilo[other], bslab[other].reshape(part_of, 2 * rank))
    got = got[:share] + got[share:]
    column = (c * nx + x) * share + lax.broadcasted_iota(jnp.int32, (share, rank), 0)
    got = jnp.where(column < qw, got[:, :rank], got[:, rank:])
    for h in range(halves):
        pt[h] = got[:, h * lanes : (h + 1) * lanes]
    for k in range(nz):
        for h in range(halves):
            for j in range(pairs):
                first = 2 * (k * pairs + j)
                zs[k, h * pairs + j] = pt[h, first : first + 2].astype(bf16)

    @pl.loop(0, nz - 1)
    def _(i):
        p = far(i)
        z_copy(3, zs.at[p], rz.at[z], p, z).start()

    rz[z] = zs[z]

    z_arrived(1, mo)
    r2 = 2 * nz
    for k in range(nz):
        wider[2 * k : 2 * k + 2, :] = mo[k, 0:2].astype(f32)
        wider[r2 + 2 * k : r2 + 2 * k + 2, :] = mo[k, 2:4].astype(f32)
    oslab[c, x] = wider[...].astype(bf16)
    x_spread(2, oslab)
    z_arrived(2, mz)
    for k in range(nz):
        wider[lr * k : lr * (k + 1), :] = mz[k].astype(f32)
    mslab[c, x] = wider[...].astype(bf16)
    x_spread(4, mslab)
    z_left(0, bz)
    z_left(1, mo)
    z_left(2, mz)
    bnat[...] = mul(by_latent, bslab[...].reshape(latent, 2 * rank)).astype(bf16)

    z_arrived(3, rz)
    proj = rz[0].astype(f32)
    for k in range(1, nz):
        proj = proj + rz[k].astype(f32)
    ag[z] = proj.astype(bf16)
    sz[z] = jnp.full((1, 128), jnp.sum(proj * proj), f32)
    z_spread(5, sz)
    z_spread(4, ag)

    x_onward(2, oslab)
    z_left(3, rz)
    x_left(0, bslab)
    for dx in range(1, nx):
        p = lax.rem(x + dx, nx)
        x_copy(1, xs.at[p], rx.at[x], dx).wait_send()
    for dx in range(nx):
        p = lax.rem(x + dx, nx)
        c_copy(1, dx, rounded.at[rows(other, p)], rc.at[p]).wait_send()
    x_arrived(2, oslab)
    by_rank = moved(2, (nz, nx, nc), back=True)
    for k, decay in enumerate((first_decay, second_decay)):
        old = oslab[:, :, k * r2 : (k + 1) * r2].reshape(rank, w)
        mold[k] = (decay * mul_t(old, by_rank)).reshape(nc, nx, share, rank)

    z_arrived(5, sz)
    sp[mine] = jnp.sum(sz[...], axis=0)

    def p_copy(src, dst, peer, there, here):
        return pltpu.make_async_remote_copy(
            src_ref=src, dst_ref=dst,
            send_sem=psend.at[there], recv_sem=precv.at[here],
            device_id=peer, device_id_type=MESH,
        )

    @pl.loop(1, plane)
    def _(i):
        peer, p = plane_peer(i)
        p_copy(sp.at[mine], sp.at[mine], peer, p, mine).start()

    z_arrived(4, ag)
    for k in range(nz):
        for h in range(halves):
            for j in range(pairs):
                first = 2 * (k * pairs + j)
                pt[h, first : first + 2] = ag[k, h * pairs + j].astype(f32)
    for h in range(halves):
        ps[c, x, :, h * lanes : (h + 1) * lanes] = pt[h].astype(bf16)
    x_spread(3, ps)
    z_left(4, ag)
    z_left(5, sz)
    x_left(2, oslab)

    x_onward(4, mslab)
    x_arrived(4, mslab)
    mnat[...] = mul(by_latent, mslab[...].reshape(latent, w)).astype(bf16)
    x_left(4, mslab)

    @pl.loop(1, plane)
    def _(i):
        peer, p = plane_peer(i)
        p_copy(sp.at[p], sp.at[p], peer, p, p).wait_recv()

    @pl.loop(1, plane)
    def _(i):
        peer, p = plane_peer(i)
        p_copy(sp.at[p], sp.at[p], peer, p, p).wait_send()

    mean = jnp.sum(sp[...], axis=0)[:, 0:1] / count + mean_guard
    scale = 1.0 / jnp.sqrt(mean)
    scale_out[...] = jnp.broadcast_to(scale, scale_out.shape)

    def settle(core, p):
        scaled = ps[core, p].astype(f32) * scale
        first_new = mold[0, core, p] + (1.0 - first_decay) * scaled
        second_new = mold[1, core, p] + (1.0 - second_decay) * scaled * scaled
        heads[core, p] = (first_new / (jnp.sqrt(second_new) + root_guard)).astype(bf16)

    settle(c, x)
    for dx in X_ORDER[nx][::-1]:
        p = lax.rem(x + dx, nx)
        x_from(3, ps.at[c, p], dx)
        c_copy(3, dx, ps.at[c, p], ps.at[c, p]).start()
    for dx in X_ORDER[nx][::-1]:
        settle(c, lax.rem(x + dx, nx))
    for dx in (0,) + X_ORDER[nx][::-1]:
        p = lax.rem(x + dx, nx)
        c_copy(3, dx, ps.at[other, p], ps.at[other, p]).wait_recv()
        settle(other, p)
    x_left(3, ps)


def moments(scaled, first_old, second_old):
    first = first_decay * first_old + (1.0 - first_decay) * scaled
    second = second_decay * second_old + (1.0 - second_decay) * scaled * scaled
    return first, second


def finish(sizes, *refs):
    (
        heads, proj, basis, master, scale, qb, qf, qs, kb, kf, ks,
        qf_out, qs_out, qstep_out, qcopy_out, kf_out, ks_out, kstep_out, kcopy_out,
    ) = refs
    nz, nx, nc, nt = sizes
    rank = qb.shape[1]
    qw = qf.shape[1]
    z, x, c, _ = (lax.axis_index(a) for a in AXES)
    own = 2 * ((z * nx + x) * nc + c) + lax.broadcasted_iota(jnp.int32, (8, rank), 0)
    mine = jnp.where(own == lax.broadcasted_iota(jnp.int32, (8, rank), 1), 1.0, 0.0).astype(bf16)
    scaled = mul_by_t(mine, proj[...])[:2] * scale[:, 0:1]
    qf_out[...], qs_out[...] = moments(scaled[:, :qw], qf[...], qs[...])
    kf_out[...], ks_out[...] = moments(scaled[:, qw:], kf[...], ks[...])
    q_dir = heads[:qw]
    k_dir = heads[qw:]
    qstep_out[...] = mul_by_t(qb[...], q_dir)
    kstep_out[...] = mul_by_t(kb[...], k_dir)
    q_step = mul_by_t(basis[:, :rank], q_dir)
    qcopy_out[...] = (master[:, :qw].astype(f32) - step_size * q_step).astype(bf16)
    k_step = mul_by_t(basis[:, rank:], k_dir)
    kcopy_out[...] = (master[:, qw:].astype(f32) - step_size * k_step).astype(bf16)


X_ORDER = {2: (1,), 4: (2, 1, 3)}


def body(sizes, *args):
    nz, nx, nc, nt = sizes
    args = [pltpu.with_memory_space_constraint(a, pltpu.HBM) for a in args]
    ql, qg, qm, qb, qf, qs, kl, kg, km, kb, kf, ks = args
    qw, kw = qg.shape[1], kg.shape[1]
    w = qw + kw
    fs = nz * nx * nc
    lr, rank = qb.shape
    latent = lr * fs
    count = float(rank * w * nt)
    plane = nx * nc * nt
    share = w // (nc * nx)
    lanes = min(128, rank)
    pieces = (nz, rank // lanes * (share // nz // 2), 2, lanes)
    vmem = pl.BlockSpec(memory_space=pltpu.VMEM)
    hbm = pl.BlockSpec(memory_space=pltpu.HBM)
    shape = jax.ShapeDtypeStruct
    heads, proj, basis, master, scale = pl.pallas_call(
        functools.partial(kernel, sizes, (qw, kw), count),
        out_shape=(
            shape((nc, nx, share, rank), bf16), shape((nc, nx, share, rank), bf16),
            shape((latent, 2 * rank), bf16), shape((latent, w), bf16), shape((1, 128), f32),
        ),
        in_specs=[hbm] * 12,
        out_specs=[vmem] * 5,
        scratch_shapes=[
            pltpu.VMEM(ql.shape, bf16), pltpu.VMEM(qg.shape, bf16),
            pltpu.VMEM(kl.shape, bf16), pltpu.VMEM(kg.shape, bf16),
            *(pltpu.VMEM(a.shape, f32) for a in (qm, qf, qs, km, kf, ks)),
            pltpu.VMEM((nz, lr, 2 * rank), bf16),
            pltpu.VMEM((nz, 4, w), bf16),
            pltpu.VMEM((nz, lr, w), bf16),
            pltpu.VMEM((nc, nx, nz * lr, 2 * rank), bf16),
            pltpu.VMEM((nc, nx, nz * 4, w), bf16),
            pltpu.VMEM((nc, nx, nz * lr, w), bf16),
            pltpu.VMEM((w, latent), f32),
            pltpu.VMEM((w, latent), bf16),
            pltpu.VMEM((nz * lr, 2 * rank), f32),
            pltpu.VMEM((nz * lr, w), f32),
            pltpu.VMEM((2, nc, nx, share, rank), f32),
            pltpu.VMEM((nx, share, latent), bf16),
            pltpu.VMEM((nx, share, latent), bf16),
            pltpu.VMEM((nx, share, latent), bf16),
            pltpu.VMEM((nc, 2 * share, latent // nc), bf16),
            pltpu.VMEM((rank // lanes, share, lanes), f32),
            pltpu.VMEM(pieces, bf16),
            pltpu.VMEM(pieces, bf16),
            pltpu.VMEM(pieces, bf16),
            pltpu.VMEM((plane, 1, 128), f32),
            pltpu.VMEM((nz, 1, 128), f32),
            pltpu.SemaphoreType.DMA((12,)),
            pltpu.SemaphoreType.DMA((6, nz)), pltpu.SemaphoreType.DMA((6, nz)),
            pltpu.SemaphoreType.DMA((plane,)), pltpu.SemaphoreType.DMA((plane,)),
            pltpu.SemaphoreType.DMA((5, nx)), pltpu.SemaphoreType.DMA((5, nx)),
            pltpu.SemaphoreType.DMA((5, nx)), pltpu.SemaphoreType.DMA((5, nx)),
        ],
        compiler_params=pltpu.CompilerParams(
            collective_id=0, has_side_effects=True, vmem_limit_bytes=36 * 1024 * 1024
        ),
    )(*args)
    return pl.pallas_call(
        functools.partial(finish, sizes),
        out_shape=(
            shape(qf.shape, f32), shape(qs.shape, f32), shape(qm.shape, f32), shape((latent, qw), bf16),
            shape(kf.shape, f32), shape(ks.shape, f32), shape(km.shape, f32), shape((latent, kw), bf16),
        ),
        in_specs=[vmem] * 11,
        out_specs=[vmem] * 8,
        compiler_params=pltpu.CompilerParams(vmem_limit_bytes=20 * 1024 * 1024),
    )(heads.reshape(w, rank), proj.reshape(w, rank), basis, master, scale, qb, qf, qs, kb, kf, ks)


def solution(mesh, chips=(16, 4, 2)):
    nt = mesh.shape["tp"]
    finer = Mesh(mesh.devices.reshape(*chips, nt), AXES)
    in_specs = (P(FS, None), P(FS, "t"), P(FS, "t"), P(FS, None), P(FS, "t"), P(FS, "t")) * 2
    out_specs = (P(FS, "t"), P(FS, "t"), P(FS, "t"), P(None, "t")) * 2
    return jax.shard_map(
        functools.partial(body, (*chips, nt)), mesh=finer, in_specs=in_specs, out_specs=out_specs, check_vma=False
    )
```

time: 76.4 us -> 63.4 us (0.83)
  Pallas kernels: 75.6 us -> 62.6 us
    pallas_call x1, Pallas kernels: 73.2 us -> 60 us  [body(): pl.pallas_call(functools.partial(kernel, sizes, (qw, kw), count), out_sha...]
where the time goes in v3:
time: 63.4 us; the launch traced here: 63.3 us
  Pallas kernels  62.6 us (99%)
  between operations  0.64 us (1%)
    pallas_call x1, Pallas kernels, body(): pl.pallas_call(functools.partial(kernel, sizes, (qw, kw), count), out_sha...  60 us
    pallas_call x1, Pallas kernels, body(): pl.pallas_call(functools.partial(finish, sizes), out_shape=(shape(qf.shap...  2.58 us

profile of v3, /device:TPU:1, one launch (start us, length us, event | category | flops | bytes accessed | tf_op | source)
XLA Modules:
  0.0 63.3 jit_solution(15983946810897383342)
XLA Ops:
  0.6 60.0 %shard_map.179 = (bf16[2,4,160,256]{3,2,1,0:T(8,128)(2,1)S(1)}, bf16[2,4,160,256]{3,2,1,0:T(8,128)(2,1)S(1)}, bf16[512,512]{1,0:T(8,128)(2,1)S(1)}, bf16[512,1280]{1,0:T(8,128)(2,1)S(1)}, f32[1,128]{1,0:T(1,128)S(1)}) custom-call(bf16[768,512]{1,0:T(8,128)(2,1)} %refs_0_.1, bf16[768,768]{1,0:T(8,128)(2,1)} %refs_1_.1, f32[4,768]{1,0:T(4,128)} %refs_2_.1, ...), custom_call_target="tpu_custom_call" | custom-call | tf_op jit(solution)/shard_map/pallas_call | solution.py:418
  60.7 2.6 %shard_map.180 = (f32[2,768]{1,0:T(2,128)}, f32[2,768]{1,0:T(2,128)}, f32[4,768]{1,0:T(4,128)}, bf16[512,768]{1,0:T(8,128)(2,1)}, f32[2,512]{1,0:T(2,128)}, /*in...) custom-call(bf16[1280,256]{1,0:T(8,128)(2,1)S(1)} %bitcast.2, bf16[1280,256]{1,0:T(8,128)(2,1)S(1)} %bitcast.3, ...), custom_call_target="tpu_custom_call" | custom-call | tf_op jit(solution)/shard_map/pallas_call | solution.py:461

commit v4 on v3

--- a/solution.py
+++ b/solution.py
@@ -60,9 +60,9 @@
     qw, kw = widths
     (
         ql, qg, qm_h, qb, qf_h, qs_h, kl, kg, km_h, kb, kf_h, ks_h,
-        heads, ps, bnat, mnat, scale_out,
-        ql_v, qg_v, kl_v, kg_v, qm, qf, qs, km, kf, ks,
-        bz, mo, mz, bslab, oslab, mslab, tokens, rounded, wide, wider, mold,
+        heads, ps, bnat, mnat, scale_out, qb_v, qf, qs, kb_v, kf, ks,
+        ql_v, qg_v, kl_v, kg_v, qm, km,
+        bz, mm, bslab, oslab, mslab, tokens, rounded, wide, wider, mold,
         rc, xs, rx, hilo, pt, zs, rz, ag, sp, sz,
         load_sem, zsend, zrecv, psend, precv, xsend, xrecv, csend, crecv,
     ) = refs
@@ -83,54 +83,43 @@
             (ql, ql_v), (qg, qg_v), (kl, kl_v), (kg, kg_v),
             (qb, bz.at[z, :, :rank]), (kb, bz.at[z, :, rank:]),
             (qf_h, qf), (qs_h, qs), (kf_h, kf), (ks_h, ks), (qm_h, qm), (km_h, km),
+            (qb, qb_v), (kb, kb_v),
         ))
     ]
-    for load in loads:
-        load.start()
 
     barrier = pltpu.get_barrier_semaphore()
     plane = nx * nc * nt
     mine = (x * nc + c) * nt + t
 
-    def far(i):
-        h = (i + 1) // 2
-        return lax.rem(z + nz // 2 + h * (2 * lax.rem(i, 2) - 1) + nz, nz)
-
-    def plane_peer(i):
-        p = lax.rem(mine + i, plane)
-        return (z, p // (nc * nt), lax.rem(p // nt, nc), lax.rem(p, nt)), p
-
-    @pl.loop(0, nz - 1)
-    def _(i):
-        pl.semaphore_signal(barrier, inc=1, device_id=(far(i), x, c, t), device_id_type=MESH)
-
-    @pl.loop(1, plane)
-    def _(i):
-        pl.semaphore_signal(barrier, inc=1, device_id=plane_peer(i)[0], device_id_type=MESH)
-
-    def z_copy(stage, src, dst, peer, slot):
+    along = [nz // 2] + [nz // 2 + h * side for h in range(1, nz // 2) for side in (1, -1)]
+    peers = [lax.rem(z + d, nz) for d in along]
+    xp = [lax.rem(x + d, nx) for d in range(nx)]
+    tp = [lax.rem(t + d, nt) for d in range(nt)]
+    around = [
+        (z, xp[dx], core, tp[dt])
+        for dx in range(nx) for dt in range(nt) for core in (c, other)
+        if dx or dt or core is other
+    ]
+
+    for p in peers:
+        pl.semaphore_signal(barrier, inc=1, device_id=(p, x, c, t), device_id_type=MESH)
+    for load in loads:
+        load.start()
+    for peer in around:
+        pl.semaphore_signal(barrier, inc=1, device_id=peer, device_id_type=MESH)
+
+    def z_copy(stage, src, dst, peer):
         return pltpu.make_async_remote_copy(
-            src_ref=src, dst_ref=dst,
-            send_sem=zsend.at[stage, peer], recv_sem=zrecv.at[stage, slot],
+            src_ref=src, dst_ref=dst, send_sem=zsend.at[stage], recv_sem=zrecv.at[stage],
             device_id=(peer, x, c, t), device_id_type=MESH,
         )
 
     def z_spread(stage, buf):
-        @pl.loop(0, nz - 1)
-        def _(i):
-            z_copy(stage, buf.at[z], buf.at[z], far(i), z).start()
-
-    def z_arrived(stage, buf):
-        @pl.loop(0, nz - 1)
-        def _(i):
-            p = far(i)
-            z_copy(stage, buf.at[p], buf.at[p], p, p).wait_recv()
-
-    def z_left(stage, buf):
-        @pl.loop(0, nz - 1)
-        def _(i):
-            p = far(i)
-            z_copy(stage, buf.at[p], buf.at[p], p, p).wait_send()
+        for p in peers:
+            z_copy(stage, buf.at[z], buf.at[z], p).start()
+
+    def z_all(stage, buf, n=nz - 1):
+        return z_copy(stage, buf.at[pl.ds(0, n)], buf.at[pl.ds(0, n)], peers[0])
 
     def x_copy(stage, src, dst, dx):
         p = lax.rem(x + dx, nx)
@@ -189,12 +178,13 @@
     rounded[...] = tokens[...].astype(bf16)
     for load in loads[4:]:
         load.wait()
-    mo[z, 0:2, :qw] = qf[...].astype(bf16)
-    mo[z, 0:2, qw:] = kf[...].astype(bf16)
-    mo[z, 2:4, :qw] = qs[...].astype(bf16)
-    mo[z, 2:4, qw:] = ks[...].astype(bf16)
-    mz[z, :, :qw] = qm[...].astype(bf16)
-    mz[z, :, qw:] = km[...].astype(bf16)
+    zr, zq = lax.rem(z, 4), z // 4
+    mm[zr, zq, 0:2, :qw] = qf[...].astype(bf16)
+    mm[zr, zq, 0:2, qw:] = kf[...].astype(bf16)
+    mm[zr, zq, 2:4, :qw] = qs[...].astype(bf16)
+    mm[zr, zq, 2:4, qw:] = ks[...].astype(bf16)
+    mm[zr, zq, 4:8, :qw] = qm[...].astype(bf16)
+    mm[zr, zq, 4:8, qw:] = km[...].astype(bf16)
     pl.semaphore_wait(barrier, nz - 1 + plane - 1)
 
     order = X_ORDER[nx] + (0,)
@@ -202,8 +192,6 @@
     for dx in order:
         p = lax.rem(x + dx, nx)
         c_copy(1, dx, rounded.at[rows(other, p)], rc.at[p]).start()
-    z_spread(1, mo)
-    z_spread(2, mz)
     for dx in order:
         p = lax.rem(x + dx, nx)
         c_copy(1, dx, rc.at[p], rc.at[p]).wait_recv()
@@ -213,13 +201,20 @@
             x_copy(1, xs.at[p], rx.at[x], dx).start()
         else:
             tokens[rows(c, p)] = both
+
+    for k in range(1, nz // 4):
+        z_copy(1, mm.at[zr, zq], mm.at[zr, zq], lax.rem(z + 4 * k, nz)).start()
     by_latent = moved(lr, (nz, nx, nc))
 
-    z_arrived(0, bz)
+    z_all(0, bz).wait_recv()
     for k in range(nz):
         wide[lr * k : lr * (k + 1), :] = bz[k].astype(f32)
     bslab[c, x] = wide[...].astype(bf16)
     x_spread(0, bslab)
+    if nz > 4:
+        z_all(1, mm.at[0], nz // 4 - 1).wait_recv()
+    for d in (2, 1, nz - 1):
+        z_copy(2, mm.at[zr], mm.at[zr], lax.rem(z + d, nz)).start()
 
     total = tokens[rows(c, x)]
     for dx in range(1, nx):
@@ -250,41 +245,38 @@
                 first = 2 * (k * pairs + j)
                 zs[k, h * pairs + j] = pt[h, first : first + 2].astype(bf16)
 
-    @pl.loop(0, nz - 1)
-    def _(i):
-        p = far(i)
-        z_copy(3, zs.at[p], rz.at[z], p, z).start()
-
+    for p in peers:
+        z_copy(3, zs.at[p], rz.at[z], p).start()
     rz[z] = zs[z]
 
-    z_arrived(1, mo)
+    z_all(2, mm, 3).wait_recv()
     r2 = 2 * nz
     for k in range(nz):
-        wider[2 * k : 2 * k + 2, :] = mo[k, 0:2].astype(f32)
-        wider[r2 + 2 * k : r2 + 2 * k + 2, :] = mo[k, 2:4].astype(f32)
+        wider[2 * k : 2 * k + 2, :] = mm[k % 4, k // 4, 0:2].astype(f32)
+        wider[r2 + 2 * k : r2 + 2 * k + 2, :] = mm[k % 4, k // 4, 2:4].astype(f32)
     oslab[c, x] = wider[...].astype(bf16)
     x_spread(2, oslab)
-    z_arrived(2, mz)
     for k in range(nz):
-        wider[lr * k : lr * (k + 1), :] = mz[k].astype(f32)
+        wider[lr * k : lr * (k + 1), :] = mm[k % 4, k // 4, 4:8].astype(f32)
     mslab[c, x] = wider[...].astype(bf16)
     x_spread(4, mslab)
-    z_left(0, bz)
-    z_left(1, mo)
-    z_left(2, mz)
+    z_all(0, bz).wait_send()
+    if nz > 4:
+        z_all(1, mm.at[0], nz // 4 - 1).wait_send()
+    z_all(2, mm, 3).wait_send()
     bnat[...] = mul(by_latent, bslab[...].reshape(latent, 2 * rank)).astype(bf16)
 
-    z_arrived(3, rz)
+    z_all(3, rz).wait_recv()
     proj = rz[0].astype(f32)
     for k in range(1, nz):
         proj = proj + rz[k].astype(f32)
     ag[z] = proj.astype(bf16)
     sz[z] = jnp.full((1, 128), jnp.sum(proj * proj), f32)
+    z_spread(4, ag)
     z_spread(5, sz)
-    z_spread(4, ag)
 
     x_onward(2, oslab)
-    z_left(3, rz)
+    z_all(3, zs).wait_send()
     x_left(0, bslab)
     for dx in range(1, nx):
         p = lax.rem(x + dx, nx)
@@ -298,22 +290,19 @@
         old = oslab[:, :, k * r2 : (k + 1) * r2].reshape(rank, w)
         mold[k] = (decay * mul_t(old, by_rank)).reshape(nc, nx, share, rank)
 
-    z_arrived(5, sz)
+    z_all(5, sz).wait_recv()
     sp[mine] = jnp.sum(sz[...], axis=0)
 
-    def p_copy(src, dst, peer, there, here):
+    def p_copy(src, dst, peer):
         return pltpu.make_async_remote_copy(
-            src_ref=src, dst_ref=dst,
-            send_sem=psend.at[there], recv_sem=precv.at[here],
+            src_ref=src, dst_ref=dst, send_sem=psend.at[0], recv_sem=precv.at[0],
             device_id=peer, device_id_type=MESH,
         )
 
-    @pl.loop(1, plane)
-    def _(i):
-        peer, p = plane_peer(i)
-        p_copy(sp.at[mine], sp.at[mine], peer, p, mine).start()
-
-    z_arrived(4, ag)
+    for peer in around:
+        p_copy(sp.at[mine], sp.at[mine], peer).start()
+
+    z_all(4, ag).wait_recv()
     for k in range(nz):
         for h in range(halves):
             for j in range(pairs):
@@ -322,8 +311,8 @@
     for h in range(halves):
         ps[c, x, :, h * lanes : (h + 1) * lanes] = pt[h].astype(bf16)
     x_spread(3, ps)
-    z_left(4, ag)
-    z_left(5, sz)
+    z_all(4, ag).wait_send()
+    z_all(5, sz).wait_send()
     x_left(2, oslab)
 
     x_onward(4, mslab)
@@ -331,15 +320,9 @@
     mnat[...] = mul(by_latent, mslab[...].reshape(latent, w)).astype(bf16)
     x_left(4, mslab)
 
-    @pl.loop(1, plane)
-    def _(i):
-        peer, p = plane_peer(i)
-        p_copy(sp.at[p], sp.at[p], peer, p, p).wait_recv()
-
-    @pl.loop(1, plane)
-    def _(i):
-        peer, p = plane_peer(i)
-        p_copy(sp.at[p], sp.at[p], peer, p, p).wait_send()
+    everyone = sp.at[pl.ds(0, plane - 1)]
+    p_copy(everyone, everyone, around[0]).wait_recv()
+    p_copy(everyone, everyone, around[0]).wait_send()
 
     mean = jnp.sum(sp[...], axis=0)[:, 0:1] / count + mean_guard
     scale = 1.0 / jnp.sqrt(mean)
@@ -375,24 +358,36 @@
     (
         heads, proj, basis, master, scale, qb, qf, qs, kb, kf, ks,
         qf_out, qs_out, qstep_out, qcopy_out, kf_out, ks_out, kstep_out, kcopy_out,
+        fresh_q, fresh_k, sems,
     ) = refs
     nz, nx, nc, nt = sizes
     rank = qb.shape[1]
     qw = qf.shape[1]
     z, x, c, _ = (lax.axis_index(a) for a in AXES)
+    q_dir = heads[:qw]
+    k_dir = heads[qw:]
+    latent = basis.shape[0]
+    cut = latent // 2
+    copies = []
+    for columns, towards, old, fresh, out in (
+        (slice(0, rank), q_dir, slice(0, qw), fresh_q, qcopy_out),
+        (slice(rank, 2 * rank), k_dir, slice(qw, master.shape[1]), fresh_k, kcopy_out),
+    ):
+        for k in range(2):
+            some = slice(k * cut, (k + 1) * cut)
+            step = mul_by_t(basis[some, columns], towards)
+            fresh[some] = (master[some, old].astype(f32) - step_size * step).astype(bf16)
+            copies.append(pltpu.make_async_copy(fresh.at[some], out.at[some], sems.at[len(copies)]))
+            copies[-1].start()
     own = 2 * ((z * nx + x) * nc + c) + lax.broadcasted_iota(jnp.int32, (8, rank), 0)
     mine = jnp.where(own == lax.broadcasted_iota(jnp.int32, (8, rank), 1), 1.0, 0.0).astype(bf16)
     scaled = mul_by_t(mine, proj[...])[:2] * scale[:, 0:1]
     qf_out[...], qs_out[...] = moments(scaled[:, :qw], qf[...], qs[...])
     kf_out[...], ks_out[...] = moments(scaled[:, qw:], kf[...], ks[...])
-    q_dir = heads[:qw]
-    k_dir = heads[qw:]
     qstep_out[...] = mul_by_t(qb[...], q_dir)
     kstep_out[...] = mul_by_t(kb[...], k_dir)
-    q_step = mul_by_t(basis[:, :rank], q_dir)
-    qcopy_out[...] = (master[:, :qw].astype(f32) - step_size * q_step).astype(bf16)
-    k_step = mul_by_t(basis[:, rank:], k_dir)
-    kcopy_out[...] = (master[:, qw:].astype(f32) - step_size * k_step).astype(bf16)
+    for copy in copies:
+        copy.wait()
 
 
 X_ORDER = {2: (1,), 4: (2, 1, 3)}
@@ -415,21 +410,21 @@
     vmem = pl.BlockSpec(memory_space=pltpu.VMEM)
     hbm = pl.BlockSpec(memory_space=pltpu.HBM)
     shape = jax.ShapeDtypeStruct
-    heads, proj, basis, master, scale = pl.pallas_call(
+    heads, proj, basis, master, scale, *small = pl.pallas_call(
         functools.partial(kernel, sizes, (qw, kw), count),
         out_shape=(
             shape((nc, nx, share, rank), bf16), shape((nc, nx, share, rank), bf16),
             shape((latent, 2 * rank), bf16), shape((latent, w), bf16), shape((1, 128), f32),
+            *(shape(a.shape, a.dtype) for a in (qb, qf, qs, kb, kf, ks)),
         ),
         in_specs=[hbm] * 12,
-        out_specs=[vmem] * 5,
+        out_specs=[vmem] * 11,
         scratch_shapes=[
             pltpu.VMEM(ql.shape, bf16), pltpu.VMEM(qg.shape, bf16),
             pltpu.VMEM(kl.shape, bf16), pltpu.VMEM(kg.shape, bf16),
-            *(pltpu.VMEM(a.shape, f32) for a in (qm, qf, qs, km, kf, ks)),
+            *(pltpu.VMEM(a.shape, f32) for a in (qm, km)),
             pltpu.VMEM((nz, lr, 2 * rank), bf16),
-            pltpu.VMEM((nz, 4, w), bf16),
-            pltpu.VMEM((nz, lr, w), bf16),
+            pltpu.VMEM((4, nz // 4, 8, w), bf16),
             pltpu.VMEM((nc, nx, nz * lr, 2 * rank), bf16),
             pltpu.VMEM((nc, nx, nz * 4, w), bf16),
             pltpu.VMEM((nc, nx, nz * lr, w), bf16),
@@ -448,9 +443,9 @@
             pltpu.VMEM(pieces, bf16),
             pltpu.VMEM((plane, 1, 128), f32),
             pltpu.VMEM((nz, 1, 128), f32),
-            pltpu.SemaphoreType.DMA((12,)),
-            pltpu.SemaphoreType.DMA((6, nz)), pltpu.SemaphoreType.DMA((6, nz)),
-            pltpu.SemaphoreType.DMA((plane,)), pltpu.SemaphoreType.DMA((plane,)),
+            pltpu.SemaphoreType.DMA((14,)),
+            pltpu.SemaphoreType.DMA((6,)), pltpu.SemaphoreType.DMA((6,)),
+            pltpu.SemaphoreType.DMA((1,)), pltpu.SemaphoreType.DMA((1,)),
             pltpu.SemaphoreType.DMA((5, nx)), pltpu.SemaphoreType.DMA((5, nx)),
             pltpu.SemaphoreType.DMA((5, nx)), pltpu.SemaphoreType.DMA((5, nx)),
         ],
@@ -465,9 +460,12 @@
             shape(kf.shape, f32), shape(ks.shape, f32), shape(km.shape, f32), shape((latent, kw), bf16),
         ),
         in_specs=[vmem] * 11,
-        out_specs=[vmem] * 8,
+        out_specs=[vmem, vmem, vmem, hbm] * 2,
+        scratch_shapes=[
+            pltpu.VMEM((latent, qw), bf16), pltpu.VMEM((latent, kw), bf16), pltpu.SemaphoreType.DMA((4,)),
+        ],
         compiler_params=pltpu.CompilerParams(vmem_limit_bytes=20 * 1024 * 1024),
-    )(heads.reshape(w, rank), proj.reshape(w, rank), basis, master, scale, qb, qf, qs, kb, kf, ks)
+    )(heads.reshape(w, rank), proj.reshape(w, rank), basis, master, scale, *small)
 
 
 def solution(mesh, chips=(16, 4, 2)):

time: 63.4 us -> 60.8 us (0.959)
  Pallas kernels: 62.6 us -> 60 us
    pallas_call x1, Pallas kernels: 60 us -> 58 us  [body(): pl.pallas_call(functools.partial(kernel, sizes, (qw, kw), count), out_sha...]
where the time goes in v4:
time: 60.8 us; the launch traced here: 60.7 us
  Pallas kernels  60 us (99%)
  between operations  0.65 us (1%)
    pallas_call x1, Pallas kernels, body(): pl.pallas_call(functools.partial(kernel, sizes, (qw, kw), count), out_sha...  58 us
    pallas_call x1, Pallas kernels, body(): pl.pallas_call(functools.partial(finish, sizes), out_shape=(shape(qf.shap...  2.05 us

profile of v4, /device:TPU:1, one launch (start us, length us, event | category | flops | bytes accessed | tf_op | source)
XLA Modules:
  0.0 60.7 jit_solution(5049409454628346842)
XLA Ops:
  0.6 58.0 %shard_map.179 = (bf16[2,4,160,256]{3,2,1,0:T(8,128)(2,1)S(1)}, bf16[2,4,160,256]{3,2,1,0:T(8,128)(2,1)S(1)}, bf16[512,512]{1,0:T(8,128)(2,1)S(1)}, bf16[512,128...) custom-call(bf16[768,512]{1,0:T(8,128)(2,1)} %refs_0_.1, ...), custom_call_target="tpu_custom_call" | custom-call | tf_op jit(solution)/shard_map/pallas_call | solution.py:413
  58.6 2.1 %shard_map.180 = (f32[2,768]{1,0:T(2,128)}, f32[2,768]{1,0:T(2,128)}, f32[4,768]{1,0:T(4,128)}, bf16[512,768]{1,0:T(8,128)(2,1)}, f32[2,512]{1,0:T(2,128)}, /*in...) custom-call(bf16[1280,256]{1,0:T(8,128)(2,1)S(1)} %bitcast.2, bf16[1280,256]{1,0:T(8,128)(2,1)S(1)} %bitcast.3, ...), custom_call_target="tpu_custom_call" | custom-call | tf_op jit(solution)/shard_map/pallas_call | solution.py:456

commit v5 on v4

--- a/solution.py
+++ b/solution.py
@@ -63,8 +63,8 @@
         heads, ps, bnat, mnat, scale_out, qb_v, qf, qs, kb_v, kf, ks,
         ql_v, qg_v, kl_v, kg_v, qm, km,
         bz, mm, bslab, oslab, mslab, tokens, rounded, wide, wider, mold,
-        rc, xs, rx, hilo, pt, zs, rz, ag, sp, sz,
-        load_sem, zsend, zrecv, psend, precv, xsend, xrecv, csend, crecv,
+        rc, xs, rx, relay, hilo, pt, zs, rz, ag, sp, sz,
+        load_sem, zsend, zrecv, psend, precv, xsend, xrecv, csend, crecv, rsend, rrecv, bsend, brecv,
     ) = refs
     w = qw + kw
     rank = qb.shape[1]
@@ -125,16 +125,26 @@
         p = lax.rem(x + dx, nx)
         return pltpu.make_async_remote_copy(
             src_ref=src, dst_ref=dst,
-            send_sem=xsend.at[stage, dx], recv_sem=xrecv.at[stage, nx - dx],
+            send_sem=xsend.at[stage // 3, dx], recv_sem=xrecv.at[stage // 3, nx - dx],
             device_id=(z, p, c, t), device_id_type=MESH,
         )
 
     def x_from(stage, buf, dx):
         pltpu.make_async_remote_copy(
             src_ref=buf, dst_ref=buf,
-            send_sem=xsend.at[stage, dx], recv_sem=xrecv.at[stage, dx],
+            send_sem=xsend.at[stage // 3, dx], recv_sem=xrecv.at[stage // 3, dx],
             device_id=(z, lax.rem(x + dx, nx), c, t), device_id_type=MESH,
         ).wait_recv()
+
+    right, across, left = xp[1], xp[2], xp[3]
+    half = share // 2
+    ahead, behind = pl.ds(0, half), pl.ds(half, half)
+
+    def beside(sends, recvs, k, rightward, src, dst):
+        return pltpu.make_async_remote_copy(
+            src_ref=src, dst_ref=dst, send_sem=sends.at[k], recv_sem=recvs.at[k],
+            device_id=(z, right if rightward else left, c, t), device_id_type=MESH,
+        )
 
     def c_copy(stage, k, src, dst):
         return pltpu.make_async_remote_copy(
@@ -192,35 +202,57 @@
     for dx in order:
         p = lax.rem(x + dx, nx)
         c_copy(1, dx, rounded.at[rows(other, p)], rc.at[p]).start()
+
+    sums = (
+        beside(rsend, rrecv, 0, True, xs.at[across, ahead], relay.at[0]),
+        beside(rsend, rrecv, 1, False, xs.at[across, behind], relay.at[1]),
+        beside(rsend, rrecv, 2, True, xs.at[right, behind], rx.at[0, behind]),
+        beside(rsend, rrecv, 3, False, xs.at[left, ahead], rx.at[1, ahead]),
+        beside(rsend, rrecv, 4, True, xs.at[right, ahead], rx.at[0, ahead]),
+        beside(rsend, rrecv, 5, False, xs.at[left, behind], rx.at[1, behind]),
+    )
     for dx in order:
-        p = lax.rem(x + dx, nx)
+        p = xp[dx]
         c_copy(1, dx, rc.at[p], rc.at[p]).wait_recv()
         both = tokens[rows(c, p)] + rc[p].astype(f32)
-        if dx:
+        if dx == 2:
             xs[p] = both.astype(bf16)
-            x_copy(1, xs.at[p], rx.at[x], dx).start()
+            sums[0].start()
+            sums[1].start()
+        elif dx == 1:
+            xs[p, half:] = both[half:].astype(bf16)
+            sums[2].start()
+            tokens[rows(c, p)] = both
+        elif dx == 3:
+            xs[p, :half] = both[:half].astype(bf16)
+            sums[3].start()
+            tokens[rows(c, p)] = both
         else:
             tokens[rows(c, p)] = both
 
     for k in range(1, nz // 4):
         z_copy(1, mm.at[zr, zq], mm.at[zr, zq], lax.rem(z + 4 * k, nz)).start()
     by_latent = moved(lr, (nz, nx, nc))
+
+    sums[0].wait_recv()
+    passed = tokens[rows(c, right)]
+    xs[right, :half] = (passed[:half] + relay[0].astype(f32)).astype(bf16)
+    sums[4].start()
+    sums[1].wait_recv()
+    passed = tokens[rows(c, left)]
+    xs[left, half:] = (passed[half:] + relay[1].astype(f32)).astype(bf16)
+    sums[5].start()
 
     z_all(0, bz).wait_recv()
     for k in range(nz):
         wide[lr * k : lr * (k + 1), :] = bz[k].astype(f32)
     bslab[c, x] = wide[...].astype(bf16)
     x_spread(0, bslab)
-    if nz > 4:
-        z_all(1, mm.at[0], nz // 4 - 1).wait_recv()
-    for d in (2, 1, nz - 1):
-        z_copy(2, mm.at[zr], mm.at[zr], lax.rem(z + d, nz)).start()
 
     total = tokens[rows(c, x)]
-    for dx in range(1, nx):
-        p = lax.rem(x + dx, nx)
-        x_from(1, rx.at[p], dx)
-        total = total + rx[p].astype(f32)
+    for k in range(2, 6):
+        sums[k].wait_recv()
+    total = total + rx[0].astype(f32) + rx[1].astype(f32)
     high = total.astype(bf16)
     low = (total - high.astype(f32)).astype(bf16)
     part_of = latent // nc
@@ -229,6 +261,16 @@
     for k in range(nc):
         hilo[k, :share] = turned_high[:, k * part_of : (k + 1) * part_of]
         hilo[k, share:] = turned_low[:, k * part_of : (k + 1) * part_of]
+
+    fours = nz // 4
+    if fours > 1:
+        z_all(1, mm.at[0], fours - 1).wait_recv()
+    for d, some in (
+        (2, pl.ds(0, (fours + 1) // 2)), (nz - 2, pl.ds((fours + 1) // 2, fours // 2)),
+        (1, pl.ds(0, fours)), (nz - 1, pl.ds(0, fours)),
+    ):
+        if some.size:
+            z_copy(2, mm.at[zr, some], mm.at[zr, some], lax.rem(z + d, nz)).start()
 
     x_onward(0, bslab)
     got = mul(hilo[c], bslab[c].reshape(part_of, 2 * rank))
@@ -255,11 +297,37 @@
         wider[2 * k : 2 * k + 2, :] = mm[k % 4, k // 4, 0:2].astype(f32)
         wider[r2 + 2 * k : r2 + 2 * k + 2, :] = mm[k % 4, k // 4, 2:4].astype(f32)
     oslab[c, x] = wider[...].astype(bf16)
-    x_spread(2, oslab)
     for k in range(nz):
         wider[lr * k : lr * (k + 1), :] = mm[k % 4, k // 4, 4:8].astype(f32)
     mslab[c, x] = wider[...].astype(bf16)
-    x_spread(4, mslab)
+    bulk = (
+        beside(bsend, brecv, 0, True, oslab.at[c, x], oslab.at[c, x]),
+        beside(bsend, brecv, 1, False, mslab.at[c, x], mslab.at[c, x]),
+        beside(bsend, brecv, 2, True, mslab.at[c, x], mslab.at[c, x]),
+        beside(bsend, brecv, 3, False, oslab.at[c, x], oslab.at[c, x]),
+        beside(bsend, brecv, 4, True, oslab.at[c, left], oslab.at[c, left]),
+        beside(bsend, brecv, 5, False, mslab.at[c, right], mslab.at[c, right]),
+    )
+    landing = (
+        (0, True, oslab, left, 3), (1, False, mslab, right, 1), (2, True, mslab, left, 3),
+        (3, False, oslab, right, 1), (4, True, oslab, across, 2), (5, False, mslab, across, 2),
+    )
+
+    def c_bulk(slabs, dx, p):
+        return c_copy(2 if slabs is oslab else 4, dx, slabs.at[c, p], slabs.at[c, p])
+
+    def bulk_onward(which):
+        for k in which:
+            _, rightward, slabs, p, dx = landing[k]
+            beside(bsend, brecv, k, rightward, slabs.at[c, p], slabs.at[c, p]).wait_recv()
+            if k < 2:
+                bulk[4 + k].start()
+            c_bulk(slabs, dx, p).start()
+
+    for copy in bulk[:4]:
+        copy.start()
+    c_bulk(oslab, 0, x).start()
+    c_bulk(mslab, 0, x).start()
     z_all(0, bz).wait_send()
     if nz > 4:
         z_all(1, mm.at[0], nz // 4 - 1).wait_send()
@@ -275,20 +343,15 @@
     z_spread(4, ag)
     z_spread(5, sz)
 
-    x_onward(2, oslab)
+    bulk_onward((0, 1, 2, 3))
     z_all(3, zs).wait_send()
     x_left(0, bslab)
-    for dx in range(1, nx):
-        p = lax.rem(x + dx, nx)
-        x_copy(1, xs.at[p], rx.at[x], dx).wait_send()
+    for copy in sums:
+        copy.wait_send()
     for dx in range(nx):
-        p = lax.rem(x + dx, nx)
+        p = xp[dx]
         c_copy(1, dx, rounded.at[rows(other, p)], rc.at[p]).wait_send()
-    x_arrived(2, oslab)
     by_rank = moved(2, (nz, nx, nc), back=True)
-    for k, decay in enumerate((first_decay, second_decay)):
-        old = oslab[:, :, k * r2 : (k + 1) * r2].reshape(rank, w)
-        mold[k] = (decay * mul_t(old, by_rank)).reshape(nc, nx, share, rank)
 
     z_all(5, sz).wait_recv()
     sp[mine] = jnp.sum(sz[...], axis=0)
@@ -313,12 +376,19 @@
     x_spread(3, ps)
     z_all(4, ag).wait_send()
     z_all(5, sz).wait_send()
-    x_left(2, oslab)
-
-    x_onward(4, mslab)
+
+    bulk_onward((4, 5))
+    x_arrived(2, oslab)
+    for k, decay in enumerate((first_decay, second_decay)):
+        old = oslab[:, :, k * r2 : (k + 1) * r2].reshape(rank, w)
+        mold[k] = (decay * mul_t(old, by_rank)).reshape(nc, nx, share, rank)
     x_arrived(4, mslab)
     mnat[...] = mul(by_latent, mslab[...].reshape(latent, w)).astype(bf16)
-    x_left(4, mslab)
+    for copy in bulk:
+        copy.wait_send()
+    for dx in range(nx):
+        c_bulk(oslab, dx, xp[dx]).wait_send()
+        c_bulk(mslab, dx, xp[dx]).wait_send()
 
     everyone = sp.at[pl.ds(0, plane - 1)]
     p_copy(everyone, everyone, around[0]).wait_recv()
@@ -358,7 +428,7 @@
     (
         heads, proj, basis, master, scale, qb, qf, qs, kb, kf, ks,
         qf_out, qs_out, qstep_out, qcopy_out, kf_out, ks_out, kstep_out, kcopy_out,
-        fresh_q, fresh_k, sems,
+        fresh_q, fresh_k, first_q, second_q, step_q, first_k, second_k, step_k, sems,
     ) = refs
     nz, nx, nc, nt = sizes
     rank = qb.shape[1]
@@ -369,23 +439,32 @@
     latent = basis.shape[0]
     cut = latent // 2
     copies = []
-    for columns, towards, old, fresh, out in (
-        (slice(0, rank), q_dir, slice(0, qw), fresh_q, qcopy_out),
-        (slice(rank, 2 * rank), k_dir, slice(qw, master.shape[1]), fresh_k, kcopy_out),
-    ):
+
+    def send(src, dst):
+        copies.append(pltpu.make_async_copy(src, dst, sems.at[len(copies)]))
+        copies[-1].start()
+
+    def renew(columns, towards, old, fresh, out):
         for k in range(2):
             some = slice(k * cut, (k + 1) * cut)
             step = mul_by_t(basis[some, columns], towards)
             fresh[some] = (master[some, old].astype(f32) - step_size * step).astype(bf16)
-            copies.append(pltpu.make_async_copy(fresh.at[some], out.at[some], sems.at[len(copies)]))
-            copies[-1].start()
+            send(fresh.at[some], out.at[some])
+
+    renew(slice(0, rank), q_dir, slice(0, qw), fresh_q, qcopy_out)
     own = 2 * ((z * nx + x) * nc + c) + lax.broadcasted_iota(jnp.int32, (8, rank), 0)
     mine = jnp.where(own == lax.broadcasted_iota(jnp.int32, (8, rank), 1), 1.0, 0.0).astype(bf16)
     scaled = mul_by_t(mine, proj[...])[:2] * scale[:, 0:1]
-    qf_out[...], qs_out[...] = moments(scaled[:, :qw], qf[...], qs[...])
-    kf_out[...], ks_out[...] = moments(scaled[:, qw:], kf[...], ks[...])
-    qstep_out[...] = mul_by_t(qb[...], q_dir)
-    kstep_out[...] = mul_by_t(kb[...], k_dir)
+    first_q[...], second_q[...] = moments(scaled[:, :qw], qf[...], qs[...])
+    first_k[...], second_k[...] = moments(scaled[:, qw:], kf[...], ks[...])
+    step_q[...] = mul_by_t(qb[...], q_dir)
+    step_k[...] = mul_by_t(kb[...], k_dir)
+    for src, dst in (
+        (first_q, qf_out), (second_q, qs_out), (step_q, qstep_out),
+        (first_k, kf_out), (second_k, ks_out), (step_k, kstep_out),
+    ):
+        send(src, dst)
+    renew(slice(rank, 2 * rank), k_dir, slice(qw, master.shape[1]), fresh_k, kcopy_out)
     for copy in copies:
         copy.wait()
 
@@ -435,7 +514,8 @@
             pltpu.VMEM((2, nc, nx, share, rank), f32),
             pltpu.VMEM((nx, share, latent), bf16),
             pltpu.VMEM((nx, share, latent), bf16),
-            pltpu.VMEM((nx, share, latent), bf16),
+            pltpu.VMEM((2, share, latent), bf16),
+            pltpu.VMEM((2, share // 2, latent), bf16),
             pltpu.VMEM((nc, 2 * share, latent // nc), bf16),
             pltpu.VMEM((rank // lanes, share, lanes), f32),
             pltpu.VMEM(pieces, bf16),
@@ -446,8 +526,10 @@
             pltpu.SemaphoreType.DMA((14,)),
             pltpu.SemaphoreType.DMA((6,)), pltpu.SemaphoreType.DMA((6,)),
             pltpu.SemaphoreType.DMA((1,)), pltpu.SemaphoreType.DMA((1,)),
+            pltpu.SemaphoreType.DMA((2, nx)), pltpu.SemaphoreType.DMA((2, nx)),
             pltpu.SemaphoreType.DMA((5, nx)), pltpu.SemaphoreType.DMA((5, nx)),
-            pltpu.SemaphoreType.DMA((5, nx)), pltpu.SemaphoreType.DMA((5, nx)),
+            pltpu.SemaphoreType.DMA((6,)), pltpu.SemaphoreType.DMA((6,)),
+            pltpu.SemaphoreType.DMA((6,)), pltpu.SemaphoreType.DMA((6,)),
         ],
         compiler_params=pltpu.CompilerParams(
             collective_id=0, has_side_effects=True, vmem_limit_bytes=36 * 1024 * 1024
@@ -460,9 +542,11 @@
             shape(kf.shape, f32), shape(ks.shape, f32), shape(km.shape, f32), shape((latent, kw), bf16),
         ),
         in_specs=[vmem] * 11,
-        out_specs=[vmem, vmem, vmem, hbm] * 2,
+        out_specs=[hbm] * 8,
         scratch_shapes=[
-            pltpu.VMEM((latent, qw), bf16), pltpu.VMEM((latent, kw), bf16), pltpu.SemaphoreType.DMA((4,)),
+            pltpu.VMEM((latent, qw), bf16), pltpu.VMEM((latent, kw), bf16),
+            *(pltpu.VMEM(a.shape, f32) for a in (qf, qs, qm, kf, ks, km)),
+            pltpu.SemaphoreType.DMA((10,)),
         ],
         compiler_params=pltpu.CompilerParams(vmem_limit_bytes=20 * 1024 * 1024),
     )(heads.reshape(w, rank), proj.reshape(w, rank), basis, master, scale, *small)

time: 60.8 us -> 60.5 us (level)
  no operation moved by 1% of the time
where the time goes in v5:
time: 60.5 us; the launch traced here: 60.4 us
  Pallas kernels  59.7 us (99%)
  between operations  0.65 us (1%)
    pallas_call x1, Pallas kernels, body(): pl.pallas_call(functools.partial(kernel, sizes, (qw, kw), count), out_sha...  58 us
    pallas_call x1, Pallas kernels, body(): pl.pallas_call(functools.partial(finish, sizes), out_shape=(shape(qf.shap...  1.72 us

profile of v5, /device:TPU:1, one launch (start us, length us, event | category | flops | bytes accessed | tf_op | source)
XLA Modules:
  0.0 60.4 jit_solution(9073736985176667374)
XLA Ops:
  0.6 58.0 %shard_map.179 = (bf16[2,4,160,256]{3,2,1,0:T(8,128)(2,1)S(1)}, bf16[2,4,160,256]{3,2,1,0:T(8,128)(2,1)S(1)}, bf16[512,512]{1,0:T(8,128)(2,1)S(1)}, bf16[512,128...) custom-call(bf16[768,512]{1,0:T(8,128)(2,1)} %refs_0_.1, ...), custom_call_target="tpu_custom_call" | custom-call | tf_op jit(solution)/shard_map/pallas_call | solution.py:492
  58.7 1.7 %shard_map.180 = (f32[2,768]{1,0:T(2,128)}, f32[2,768]{1,0:T(2,128)}, f32[4,768]{1,0:T(4,128)}, bf16[512,768]{1,0:T(8,128)(2,1)}, f32[2,512]{1,0:T(2,128)}, /*in...) custom-call(bf16[1280,256]{1,0:T(8,128)(2,1)S(1)} %bitcast.2, bf16[1280,256]{1,0:T(8,128)(2,1)S(1)} %bitcast.3, ...), custom_call_target="tpu_custom_call" | custom-call | tf_op jit(solution)/shard_map/pallas_call | solution.py:538

commit v6 on v5

--- a/solution.py
+++ b/solution.py
@@ -339,11 +339,24 @@
     for k in range(1, nz):
         proj = proj + rz[k].astype(f32)
     ag[z] = proj.astype(bf16)
-    sz[z] = jnp.full((1, 128), jnp.sum(proj * proj), f32)
     z_spread(4, ag)
+
+    def p_copy(src, dst, peer):
+        return pltpu.make_async_remote_copy(
+            src_ref=src, dst_ref=dst, send_sem=psend.at[0], recv_sem=precv.at[0],
+            device_id=peer, device_id_type=MESH,
+        )
+
+    sp[mine] = jnp.full((1, 128), jnp.sum(proj * proj), f32)
+    for peer in around:
+        p_copy(sp.at[mine], sp.at[mine], peer).start()
+    everyone = sp.at[pl.ds(0, plane - 1)]
+
+    bulk_onward((0, 1))
+    p_copy(everyone, everyone, around[0]).wait_recv()
+    sz[z] = jnp.sum(sp[...], axis=0)
     z_spread(5, sz)
-
-    bulk_onward((0, 1, 2, 3))
+    bulk_onward((2, 3))
     z_all(3, zs).wait_send()
     x_left(0, bslab)
     for copy in sums:
@@ -352,18 +365,6 @@
         p = xp[dx]
         c_copy(1, dx, rounded.at[rows(other, p)], rc.at[p]).wait_send()
     by_rank = moved(2, (nz, nx, nc), back=True)
-
-    z_all(5, sz).wait_recv()
-    sp[mine] = jnp.sum(sz[...], axis=0)
-
-    def p_copy(src, dst, peer):
-        return pltpu.make_async_remote_copy(
-            src_ref=src, dst_ref=dst, send_sem=psend.at[0], recv_sem=precv.at[0],
-            device_id=peer, device_id_type=MESH,
-        )
-
-    for peer in around:
-        p_copy(sp.at[mine], sp.at[mine], peer).start()
 
     z_all(4, ag).wait_recv()
     for k in range(nz):
@@ -375,7 +376,6 @@
         ps[c, x, :, h * lanes : (h + 1) * lanes] = pt[h].astype(bf16)
     x_spread(3, ps)
     z_all(4, ag).wait_send()
-    z_all(5, sz).wait_send()
 
     bulk_onward((4, 5))
     x_arrived(2, oslab)
@@ -390,11 +390,15 @@
         c_bulk(oslab, dx, xp[dx]).wait_send()
         c_bulk(mslab, dx, xp[dx]).wait_send()
 
-    everyone = sp.at[pl.ds(0, plane - 1)]
-    p_copy(everyone, everyone, around[0]).wait_recv()
     p_copy(everyone, everyone, around[0]).wait_send()
-
-    mean = jnp.sum(sp[...], axis=0)[:, 0:1] / count + mean_guard
+    for dx in X_ORDER[nx][::-1]:
+        p = lax.rem(x + dx, nx)
+        x_from(3, ps.at[c, p], dx)
+        c_copy(3, dx, ps.at[c, p], ps.at[c, p]).start()
+    z_all(5, sz).wait_send()
+    z_all(5, sz).wait_recv()
+
+    mean = jnp.sum(sz[...], axis=0)[:, 0:1] / count + mean_guard
     scale = 1.0 / jnp.sqrt(mean)
     scale_out[...] = jnp.broadcast_to(scale, scale_out.shape)
 
@@ -405,10 +409,6 @@
         heads[core, p] = (first_new / (jnp.sqrt(second_new) + root_guard)).astype(bf16)
 
     settle(c, x)
-    for dx in X_ORDER[nx][::-1]:
-        p = lax.rem(x + dx, nx)
-        x_from(3, ps.at[c, p], dx)
-        c_copy(3, dx, ps.at[c, p], ps.at[c, p]).start()
     for dx in X_ORDER[nx][::-1]:
         settle(c, lax.rem(x + dx, nx))
     for dx in (0,) + X_ORDER[nx][::-1]:

time: 60.5 us -> 58.1 us (0.960)
  Pallas kernels: 59.7 us -> 57.3 us
    pallas_call x1, Pallas kernels: 58 us -> 55.6 us  [body(): pl.pallas_call(functools.partial(kernel, sizes, (qw, kw), count), out_sha...]
where the time goes in v6:
time: 58.1 us; the launch traced here: 58 us
  Pallas kernels  57.3 us (99%)
  between operations  0.65 us (1%)
    pallas_call x1, Pallas kernels, body(): pl.pallas_call(functools.partial(kernel, sizes, (qw, kw), count), out_sha...  55.6 us
    pallas_call x1, Pallas kernels, body(): pl.pallas_call(functools.partial(finish, sizes), out_shape=(shape(qf.shap...  1.72 us

profile of v6, /device:TPU:1, one launch (start us, length us, event | category | flops | bytes accessed | tf_op | source)
XLA Modules:
  0.0 58.0 jit_solution(9113438229499148652)
XLA Ops:
  0.6 55.6 %shard_map.179 = (bf16[2,4,160,256]{3,2,1,0:T(8,128)(2,1)S(1)}, bf16[2,4,160,256]{3,2,1,0:T(8,128)(2,1)S(1)}, bf16[512,512]{1,0:T(8,128)(2,1)S(1)}, bf16[512,128...) custom-call(bf16[768,512]{1,0:T(8,128)(2,1)} %refs_0_.1, ...), custom_call_target="tpu_custom_call" | custom-call | tf_op jit(solution)/shard_map/pallas_call | solution.py:492
  56.3 1.7 %shard_map.180 = (f32[2,768]{1,0:T(2,128)}, f32[2,768]{1,0:T(2,128)}, f32[4,768]{1,0:T(4,128)}, bf16[512,768]{1,0:T(8,128)(2,1)}, f32[2,512]{1,0:T(2,128)}, /*in...) custom-call(bf16[1280,256]{1,0:T(8,128)(2,1)S(1)} %bitcast.2, bf16[1280,256]{1,0:T(8,128)(2,1)S(1)} %bitcast.3, ...), custom_call_target="tpu_custom_call" | custom-call | tf_op jit(solution)/shard_map/pallas_call | solution.py:538
